TPU v7x, 512 devices: a whole 4x4x16 slice. The times are simulated.
512 devices in a mesh: sp: 16 (over z), fs: 4 (over y), tp: 8 (over x, core).
Axes of the slice: x: 4, y: 4, z: 16, core: 2. Of those that a mesh axis runs over, the one named last changes fastest.
Arguments:
- tokens: bfloat16 [8192, 2048], P(('fs', 'sp'), 'tp'), parts along dimension 0, may hold values from -6 to 6
- norm_gain: float32 [2048], replicated, may hold values from 0.1 to 1.9
- w_recept: bfloat16 [2048, 1024], P('sp', 'tp'), may hold values from -0.125 to 0.125
- w_key_a: bfloat16 [2048, 1024], P('sp', 'tp'), may hold values from -0.125 to 0.125
- w_value_a: bfloat16 [2048, 1024], P('sp', 'tp'), may hold values from -0.125 to 0.125
- w_gate_a: bfloat16 [2048, 1024], P('sp', 'tp'), may hold values from -0.125 to 0.125
- decay_down_weight: bfloat16 [2048, 64], replicated, may hold values from -0.125 to 0.125
- decay_up_weight: bfloat16 [64, 1024], P(None, 'tp'), may hold values from -0.75 to 0.75
- rate_down_weight: bfloat16 [2048, 64], replicated, may hold values from -0.125 to 0.125
- rate_up_weight: bfloat16 [64, 1024], P(None, 'tp'), may hold values from -0.75 to 0.75
- decay_base: float32 [1024], P('tp'), may hold values from -12 to -2.5
- rate_base: float32 [1024], P('tp'), may hold values from -12 to 1
- rate_shift: float32 [8192, 16], P(('fs', 'sp'), 'tp'), parts along dimension 0, may hold values from 0 to 1.39
- jolts: float32 [8192, 16], P(('fs', 'sp'), 'tp'), parts along dimension 0, may hold values from 0 to 0.69
- group_gain: float32 [1024], P('tp'), may hold values from 0.1 to 1.9
- w_query_b: bfloat16 [2048, 1024], P('sp', 'tp'), may hold values from -0.125 to 0.125
- w_key_b: bfloat16 [2048, 1024], P('sp', 'tp'), may hold values from -0.125 to 0.125
- w_value_b: bfloat16 [2048, 1024], P('sp', 'tp'), may hold values from -0.125 to 0.125
- w_gate_b: bfloat16 [2048, 1024], P('sp', 'tp'), may hold values from -0.125 to 0.125
- score_offset: float32 [8], P('tp'), may hold values from -12 to -1
- w_out_a: bfloat16 [1024, 2048], P('tp'), may hold values from -0.125 to 0.125
- w_out_b: bfloat16 [1024, 2048], P('tp'), may hold values from -0.125 to 0.125
Outputs:
- mixed: bfloat16 [8192, 2048], P(('fs', 'sp', 'tp')), parts along dimension 0
- row_log: float32 [8192, 8], P(('fs', 'sp'), 'tp'), parts along dimension 0
There are 4 independent parts, one for each index of `fs`. A program takes and returns all parts, laid end to end along the dimension named above; an argument that names none is the same for every part. Nothing has to cross between parts.
All inputs are finite; a program needn't handle non-finite values.
Results may differ from a plain program's by a relative error of at most 0.02.
Values may be sent and summed in bfloat16 or wider, within the bound.
No kernel may reach another device: no remote copies, remote signals or barrier semaphores. Data moves between devices by JAX's collectives and lax.ppermute only.
A program may use at most 64 MiB of HBM per device.

v0:
```python
import jax
import jax.numpy as jnp
from jax import lax
from jax.sharding import PartitionSpec as P

HEAD_A = 64
HEAD_B = 128


def copy_for_each(value, axis):
    devices = lax.axis_size(axis)
    return lax.all_to_all(
        jnp.broadcast_to(value[None], (devices, *value.shape)), axis, 0, 0, tiled=True
    )


def laid_out(pieces, dim):
    pieces = jnp.moveaxis(pieces, 0, dim)
    shape = pieces.shape
    return pieces.reshape(*shape[:dim], shape[dim] * shape[dim + 1], *shape[dim + 2 :])


def collect(value, axis, dim):
    pieces = copy_for_each(value, axis)
    return laid_out(pieces, dim)


def in_one_piece(arrays, axis, dim, along):
    ends, at = ([], 0)
    for a in arrays[:-1]:
        at += a.shape[along]
        ends.append(at)
    both = jnp.concatenate(arrays, axis=along)
    return tuple(jnp.split(lax.all_gather(both, axis, axis=dim, tiled=True), ends, axis=along))


def gathered_once(value, axis):
    leaves = jax.tree.leaves(value)
    order = sorted(range(len(leaves)), key=lambda k: -leaves[k].size)
    width = (1, *leaves[order[0]].shape)[-1]
    lines = [
        jnp.pad(leaves[k].reshape(-1), (0, -leaves[k].size % width)).reshape(-1, width)
        for k in order
    ]
    both, at, found = (copy_for_each(jnp.concatenate(lines), axis), 0, {})
    for k, line in zip(order, lines):
        piece = both[:, at : at + len(line)].reshape(len(both), -1)
        found[k] = piece[:, : leaves[k].size].reshape(-1, *leaves[k].shape)
        at += len(line)
    numbers = iter(range(len(leaves)))
    return jax.tree.map(lambda _: found[next(numbers)], value)


def combined_pairwise(pieces, combine):
    while len(jax.tree.leaves(pieces)[0]) > 1:
        pieces = jax.vmap(combine)(
            *(jax.tree.map(lambda part: part[side::2], pieces) for side in (0, 1))
        )
    return jax.tree.map(lambda part: part[0], pieces)


def prefix_2(value, axis, combine, identity):
    devices, index = (lax.axis_size(axis), lax.axis_index(axis))
    passed = jnp.arange(devices) < index

    def kept(part, zero, own):
        part = jnp.where(
            passed.reshape(-1, *(1 for _ in own.shape)),
            part.astype(own.dtype),
            jnp.asarray(zero, own.dtype),
        )
        return part

    pieces = gathered_once(
        jax.tree.map(lambda part, kind: part.astype(kind), value, (jnp.bfloat16, jnp.bfloat16)),
        axis,
    )
    return combined_pairwise(jax.tree.map(kept, pieces, identity, value), combine)


def cut_along(value, dim, devices):
    before, after = (value.shape[:dim], value.shape[dim + 1 :])
    return jnp.moveaxis(value.reshape(*before, devices, -1, *after), dim, 0)


def sent_and_summed(value, axis, dim):
    devices = lax.axis_size(axis)
    pieces = lax.all_to_all(cut_along(value, dim, devices), axis, 0, 0, tiled=True)
    return jnp.sum(pieces.astype(jnp.float32), axis=0)


def combine_states(earlier, follower):
    joined = jnp.einsum("hij,hjk->hik", earlier[0], follower[0])
    carried = jnp.einsum("hij,hjk->hik", earlier[1], follower[0]) + follower[1]
    return (joined, carried)


def block_pass(stacked, pieces):
    recept_c, logs_step, keys_c, values_c, unit_c, mixing_c = pieces
    block_len = recept_c.shape[0]
    totals = jnp.cumsum(logs_step, axis=0)
    preceding = jnp.concatenate([jnp.zeros_like(totals[:1]), totals[:-1]], axis=0)
    steering = unit_c * mixing_c
    places_here = jnp.arange(block_len, dtype=jnp.int32)
    below_diag = (places_here[:, None] > places_here[None, :])[:, :, None, None]
    fading = jnp.where(
        below_diag, jnp.exp(jnp.where(below_diag, preceding[:, None] - totals[None, :], 0.0)), 0.0
    )
    unit_fade = fading * unit_c[:, None]
    weigh_keys = jnp.einsum("tjhc,jhc->htj", unit_fade, keys_c)
    weigh_steer = jnp.einsum("tjhc,jhc->htj", unit_fade, steering)
    read_fade = fading * (recept_c * jnp.exp(logs_step))[:, None]
    diagonal = jnp.eye(block_len, dtype=jnp.float32)
    read_keys = (
        jnp.einsum("tjhc,jhc->htj", read_fade, keys_c)
        + diagonal * jnp.sum(recept_c * keys_c, axis=2).T[:, :, None]
    )
    read_steer = (
        jnp.einsum("tjhc,jhc->htj", read_fade, steering)
        + diagonal * jnp.sum(recept_c * steering, axis=2).T[:, :, None]
    )
    values_wide = jnp.concatenate([jnp.zeros_like(values_c), values_c], axis=2)
    entering = jnp.einsum("thc,hrc->htr", unit_c * jnp.exp(preceding), stacked)
    entering = entering + jnp.einsum("htj,jhr->htr", weigh_keys, values_wide)
    removal = jax.scipy.linalg.solve_triangular(
        weigh_steer + diagonal, entering, lower=True, unit_diagonal=True
    )
    readout = jnp.einsum("thc,hrc->htr", recept_c * jnp.exp(totals), stacked)
    readout = readout + jnp.einsum("htj,jhr->htr", read_keys, values_wide)
    readout = readout - jnp.einsum("htj,hjr->htr", read_steer, removal)
    tail_fade = jnp.exp(totals[-1][None] - totals)
    closing = stacked * jnp.exp(totals[-1])[:, None, :]
    closing = closing + jnp.einsum("jhr,jhc->hrc", values_wide, keys_c * tail_fade)
    closing = closing - jnp.einsum("hjr,jhc->hrc", removal, steering * tail_fade)
    return (closing, jnp.transpose(readout, (1, 0, 2)))


def local(
    tokens,
    norm_gain,
    w_recept,
    w_key_a,
    w_value_a,
    w_gate_a,
    decay_down_weight,
    decay_up_weight,
    rate_down_weight,
    rate_up_weight,
    decay_base,
    rate_base,
    rate_shift,
    jolts,
    group_gain,
    w_query_b,
    w_key_b,
    w_value_b,
    w_gate_b,
    score_offset,
    w_out_a,
    w_out_b,
):
    gathered = collect(tokens, "tp", 1)
    floats = gathered.astype(jnp.float32)
    normed = (
        floats * lax.rsqrt(jnp.mean(floats * floats, axis=1, keepdims=True) + 1e-06) * norm_gain
    ).astype(jnp.bfloat16)
    row_count = normed.shape[0]
    matrices = (w_recept, w_key_a, w_value_a, w_gate_a, w_query_b, w_key_b, w_value_b, w_gate_b)
    portions = in_one_piece(
        (
            matrices[0],
            matrices[1],
            matrices[2],
            matrices[3],
            matrices[4],
            matrices[5],
            matrices[6],
            matrices[7],
        ),
        "sp",
        0,
        1,
    )
    projected = tuple(
        (jnp.dot(normed, portion, preferred_element_type=jnp.float32) for portion in portions)
    )
    recept, keys_a, values_a, gate_a, query_b, keys_b, values_b, gate_b = [
        summed.astype(jnp.bfloat16) for summed in projected
    ]
    heads_a = recept.shape[1] // HEAD_A
    decay_low = jnp.tanh(
        jnp.dot(normed, decay_down_weight, preferred_element_type=jnp.float32)
    ).astype(jnp.bfloat16)
    rate_low = jnp.dot(normed, rate_down_weight, preferred_element_type=jnp.float32).astype(
        jnp.bfloat16
    )
    preact = (
        decay_base
        + jnp.dot(decay_low, decay_up_weight, preferred_element_type=jnp.float32)
        + jnp.repeat(rate_shift, HEAD_A, axis=1)
    )
    log_decay = -jnp.exp(-jax.nn.softplus(-preact) - 0.5) - jnp.repeat(jolts, HEAD_A, axis=1)
    mixing = jax.nn.sigmoid(
        rate_base + jnp.dot(rate_low, rate_up_weight, preferred_element_type=jnp.float32)
    )

    def split_heads(matrix):
        return matrix.astype(jnp.float32).reshape(row_count, heads_a, HEAD_A)

    keys_heads = split_heads(keys_a)
    unit_keys = keys_heads * lax.rsqrt(
        jnp.sum(keys_heads * keys_heads, axis=2, keepdims=True) + 1e-06
    )
    block_len = min(32, row_count)
    block_count = row_count // block_len

    def to_blocks(matrix):
        return matrix.reshape(block_count, block_len, heads_a, HEAD_A)

    inputs = tuple(
        (
            to_blocks(matrix)
            for matrix in (
                split_heads(recept),
                log_decay.reshape(row_count, heads_a, HEAD_A),
                keys_heads,
                split_heads(values_a),
                unit_keys,
                mixing.reshape(row_count, heads_a, HEAD_A),
            )
        )
    )
    identity = jnp.broadcast_to(jnp.eye(HEAD_A, dtype=jnp.float32), (heads_a, HEAD_A, HEAD_A))
    zeros_state = jnp.zeros((heads_a, HEAD_A, HEAD_A), jnp.float32)
    closing, readout = lax.scan(
        block_pass, jnp.concatenate([identity, zeros_state], axis=1), inputs
    )
    readout = readout.reshape(row_count, heads_a, 2 * HEAD_A)
    prefix = prefix_2(
        (closing[:, :HEAD_A], closing[:, HEAD_A:]), "sp", combine_states, (identity, zeros_state)
    )
    outputs_a = readout[:, :, HEAD_A:] + jnp.einsum(
        "hvk,thk->thv", prefix[1], readout[:, :, :HEAD_A]
    )
    centered = outputs_a - jnp.mean(outputs_a, axis=2, keepdims=True)
    normal_a = centered * lax.rsqrt(jnp.mean(centered * centered, axis=2, keepdims=True) + 0.00064)
    mixed_a = (
        normal_a.reshape(row_count, -1) * group_gain * jax.nn.silu(gate_a.astype(jnp.float32))
    ).astype(jnp.bfloat16)
    heads_b = query_b.shape[1] // HEAD_B
    own_index = lax.axis_index("sp")
    places = jnp.arange(row_count, dtype=jnp.int32)
    query_place = own_index * row_count + places
    query_heads = query_b.reshape(row_count, heads_b, HEAD_B)
    factor = HEAD_B ** (-0.5)
    paired = jnp.stack(
        [keys_b.reshape(row_count, heads_b, HEAD_B), values_b.reshape(row_count, heads_b, HEAD_B)]
    )

    def attend(running, paired_piece, source):
        attended, weight_sum, survive = running
        scores = (
            jnp.einsum(
                "qhd,khd->hqk", query_heads, paired_piece[0], preferred_element_type=jnp.float32
            )
            * factor
            + score_offset[:, None, None]
        )
        causal = (source * row_count + places)[None, None, :] < query_place[None, :, None]
        keep_log = jnp.where(causal, jax.nn.log_sigmoid(-scores), 0.0)
        later_sum = (
            jnp.flip(jnp.cumsum(jnp.flip(keep_log, 2), axis=2), 2) - keep_log + survive[:, :, None]
        )
        weights = jnp.where(causal, jnp.exp(jax.nn.log_sigmoid(scores) + later_sum), 0.0)
        attended = attended + jnp.einsum(
            "hqk,khd->qhd",
            weights.astype(jnp.bfloat16),
            paired_piece[1],
            preferred_element_type=jnp.float32,
        )
        return (
            attended,
            weight_sum + jnp.sum(weights, axis=2),
            survive + jnp.sum(keep_log, axis=2),
        )

    empty_b = (
        jnp.zeros((row_count, heads_b, HEAD_B), jnp.float32),
        jnp.zeros((heads_b, row_count), jnp.float32),
        jnp.zeros((heads_b, row_count), jnp.float32),
    )
    running = attend(empty_b, paired, own_index)
    all_pairs = lax.all_gather(paired[None], "sp", axis=0, tiled=True)

    def visit_piece(rounds, holding):
        source = own_index - rounds
        chosen = lax.dynamic_index_in_dim(all_pairs, jnp.maximum(source, 0), 0, False)
        return lax.cond(
            source >= 0, lambda kept: attend(kept, chosen, source), lambda kept: kept, holding
        )

    running = lax.fori_loop(1, lax.axis_size("sp"), visit_piece, running)
    mixed_b = (running[0].reshape(row_count, -1) * jax.nn.silu(gate_b.astype(jnp.float32))).astype(
        jnp.bfloat16
    )
    row_log = jnp.log(jnp.maximum(running[1].T, 0.01))
    mixed = sent_and_summed(
        (
            jnp.dot(mixed_a, w_out_a, preferred_element_type=jnp.float32)
            + jnp.dot(mixed_b, w_out_b, preferred_element_type=jnp.float32)
        ).astype(jnp.bfloat16),
        "tp",
        0,
    )
    return (mixed.astype(jnp.bfloat16), row_log)


def solution(mesh):
    in_specs = (
        P(("fs", "sp"), "tp"),
        P(),
        P("sp", "tp"),
        P("sp", "tp"),
        P("sp", "tp"),
        P("sp", "tp"),
        P(),
        P(None, "tp"),
        P(),
        P(None, "tp"),
        P("tp"),
        P("tp"),
        P(("fs", "sp"), "tp"),
        P(("fs", "sp"), "tp"),
        P("tp"),
        P("sp", "tp"),
        P("sp", "tp"),
        P("sp", "tp"),
        P("sp", "tp"),
        P("tp"),
        P("tp", None),
        P("tp", None),
    )
    out_specs = (P(("fs", "sp", "tp"), None), P(("fs", "sp"), "tp"))
    return jax.shard_map(local, mesh=mesh, in_specs=in_specs, out_specs=out_specs, check_vma=False)
```

profile of v0, /device:TPU:504, one launch (start us, length us, event | category | flops | bytes accessed | tf_op | source)
XLA Modules:
  0.0 244.6 jit_solution(12712214649210133443)
XLA Ops:
  16.1 4.3 %all-to-all-start = ((bf16[8,128,256]{1,2,0:T(8,128)(2,1)}), bf16[8,128,256]{1,2,0:T(8,128)(2,1)S(1)}, u32[]{:S(2)}, u32[]{:S(2)}) async-start(bf16[8,128,256]{1,2,0:T(8,128)(2,1)} %broadcast_in_dim.74), calls=%async_computation | async-start | bytes 1048576 | tf_op jit(solution)/shard_map/all_to_all | solution.py:12
  22.1 8.6 %all-to-all-done = bf16[8,128,256]{1,2,0:T(8,128)(2,1)S(1)} async-done(((bf16[8,128,256]{1,2,0:T(8,128)(2,1)}), bf16[8,128,256]{1,2,0:T(8,128)(2,1)S(1)}, u32[]{:S(2)}, u32[]{:S(2)}) %all-to-all-start) | async-done | bytes 524320 | tf_op jit(solution)/shard_map/all_to_all | solution.py:12
  33.3 56.6 %all-gather.4.cloned.1.call-done = bf16[2048,1024]{1,0:T(8,128)(2,1)} async-done(((bf16[128,1024]{1,0:T(8,128)(2,1)}), bf16[2048,1024]{1,0:T(8,128)(2,1)}) %all-gather.4.cloned.1.call-update) | async-done | bytes 4194320 | tf_op jit(solution)/shard_map/all_gather | solution.py:34
  98.3 48.1 %while.30 = (s32[]{:T(128)}, f32[2,128,64]{1,2,0:T(8,128)S(1)}, f32[4,32,2,128]{3,1,0,2:T(8,128)S(1)}, f32[4,32,2,64]{3,2,1,0:T(2,128)S(1)}, bf16[4,32,2,64]{3,2...) while((s32[]{:T(128)}, f32[2,128,64]{1,2,0:T(8,128)S(1)}, ...), condition=%wide.region_6.7_spmd, body=%wide.region_2.6_spmd.sunk | while | flops 11161506 | bytes 3108997 | solution.py:235
  98.5 1.8 fusion.243
  102.6 4.9 %custom-call.8 = f32[2,1,32,32]{2,3,1,0:T(8,128)S(1)} custom-call(f32[2,1,32,32]{3,2,1,0:T(8,128)S(1)} %fusion.247), custom_call_target="InvertDiagBlocksLowerTriangular" | custom-call | tf_op jit(solution)/shard_map/while/body/eval_jaxpr/jit(_solve_triangular)/vmap()/triangular_solve | solution.py:125
  110.6 1.8 fusion.243
  114.6 4.9 %custom-call.8 = f32[2,1,32,32]{2,3,1,0:T(8,128)S(1)} custom-call(f32[2,1,32,32]{3,2,1,0:T(8,128)S(1)} %fusion.247), custom_call_target="InvertDiagBlocksLowerTriangular" | custom-call | tf_op jit(solution)/shard_map/while/body/eval_jaxpr/jit(_solve_triangular)/vmap()/triangular_solve | solution.py:125
  122.6 1.8 fusion.243
  126.6 4.9 %custom-call.8 = f32[2,1,32,32]{2,3,1,0:T(8,128)S(1)} custom-call(f32[2,1,32,32]{3,2,1,0:T(8,128)S(1)} %fusion.247), custom_call_target="InvertDiagBlocksLowerTriangular" | custom-call | tf_op jit(solution)/shard_map/while/body/eval_jaxpr/jit(_solve_triangular)/vmap()/triangular_solve | solution.py:125
  134.6 1.8 fusion.243
  138.6 4.9 %custom-call.8 = f32[2,1,32,32]{2,3,1,0:T(8,128)S(1)} custom-call(f32[2,1,32,32]{3,2,1,0:T(8,128)S(1)} %fusion.247), custom_call_target="InvertDiagBlocksLowerTriangular" | custom-call | tf_op jit(solution)/shard_map/while/body/eval_jaxpr/jit(_solve_triangular)/vmap()/triangular_solve | solution.py:125
  147.6 7.8 %all-to-all-start.1 = ((bf16[16,256,64]{1,2,0:T(8,128)(2,1)}), bf16[16,256,64]{1,2,0:T(8,128)(2,1)S(1)}, u32[]{:S(2)}, u32[]{:S(2)}) async-start(bf16[16,256,64]{1,2,0:T(8,128)(2,1)} %broadcast_in_dim.107), calls=%async_computation.1 | async-start | bytes 1048576 | tf_op jit(solution)/shard_map/all_to_all | solution.py:12
  158.9 5.9 %all-gather.6.cloned.1.call-done = bf16[32,128,1,128]{3,1,2,0:T(8,128)(2,1)} async-done(((bf16[2,128,1,128]{3,1,2,0:T(8,128)(2,1)}), bf16[32,128,1,128]{3,1,2,0:T(8,128)(2,1)}) %all-gather.6.cloned.1.call-update) | async-done | bytes 1048592 | tf_op jit(solution)/shard_map/all_gather | solution.py:293
  164.8 45.0 %while.31 = (s32[]{:T(128)}, f32[128,1,128]{0,2,1:T(8,128)S(1)}, f32[1,128]{1,0:T(1,128)S(1)}, f32[1,128]{1,0:T(1,128)S(1)}, s32[]{:T(128)}, /*index=5*/bf16[16,...) while((s32[]{:T(128)}, f32[128,1,128]{0,2,1:T(8,128)S(1)}, ...), condition=%wide.region_18.19_spmd.clone, body=%wide.region_12.18_spmd.clone.sunk | while | flops 11075848 | bytes 960331 | solution.py:302
  164.8 2.9 %conditional.3 = ((f32[128,1,128]{0,2,1:T(8,128)S(1)}, f32[1,128]{1,0:T(1,128)S(1)}, f32[1,128]{1,0:T(1,128)S(1)})) conditional(s32[]{:T(128)} %convert_element_type.212, (f32[128,1,128]{0,2,1:T(8,128)S(1)}, f32[1,128]{1,0:T(1,128)S(1)}, f32[1,128]{1,0:T(1,128)S(1)}) %tuple.100, (s32[]{:T(128)}, bf16[16,2,128,1,128]{4,2,3,1,0:T(8,128)(2,1)}, ...), branch_computations={%region_13.13_spmd, %region_14.17_spmd} | conditional | flops 11075843 | bytes 959580 | solution.py:298
  167.7 3.0 %conditional.3 = ((f32[128,1,128]{0,2,1:T(8,128)S(1)}, f32[1,128]{1,0:T(1,128)S(1)}, f32[1,128]{1,0:T(1,128)S(1)})) conditional(s32[]{:T(128)} %convert_element_type.212, (f32[128,1,128]{0,2,1:T(8,128)S(1)}, f32[1,128]{1,0:T(1,128)S(1)}, f32[1,128]{1,0:T(1,128)S(1)}) %tuple.100, (s32[]{:T(128)}, bf16[16,2,128,1,128]{4,2,3,1,0:T(8,128)(2,1)}, ...), branch_computations={%region_13.13_spmd, %region_14.17_spmd} | conditional | flops 11075843 | bytes 959580 | solution.py:298
  167.8 1.6 fusion.69
  170.7 3.0 %conditional.3 = ((f32[128,1,128]{0,2,1:T(8,128)S(1)}, f32[1,128]{1,0:T(1,128)S(1)}, f32[1,128]{1,0:T(1,128)S(1)})) conditional(s32[]{:T(128)} %convert_element_type.212, (f32[128,1,128]{0,2,1:T(8,128)S(1)}, f32[1,128]{1,0:T(1,128)S(1)}, f32[1,128]{1,0:T(1,128)S(1)}) %tuple.100, (s32[]{:T(128)}, bf16[16,2,128,1,128]{4,2,3,1,0:T(8,128)(2,1)}, ...), branch_computations={%region_13.13_spmd, %region_14.17_spmd} | conditional | flops 11075843 | bytes 959580 | solution.py:298
  170.8 1.6 fusion.69
  173.7 3.0 %conditional.3 = ((f32[128,1,128]{0,2,1:T(8,128)S(1)}, f32[1,128]{1,0:T(1,128)S(1)}, f32[1,128]{1,0:T(1,128)S(1)})) conditional(s32[]{:T(128)} %convert_element_type.212, (f32[128,1,128]{0,2,1:T(8,128)S(1)}, f32[1,128]{1,0:T(1,128)S(1)}, f32[1,128]{1,0:T(1,128)S(1)}) %tuple.100, (s32[]{:T(128)}, bf16[16,2,128,1,128]{4,2,3,1,0:T(8,128)(2,1)}, ...), branch_computations={%region_13.13_spmd, %region_14.17_spmd} | conditional | flops 11075843 | bytes 959580 | solution.py:298
  173.8 1.6 fusion.69
  176.7 3.0 %conditional.3 = ((f32[128,1,128]{0,2,1:T(8,128)S(1)}, f32[1,128]{1,0:T(1,128)S(1)}, f32[1,128]{1,0:T(1,128)S(1)})) conditional(s32[]{:T(128)} %convert_element_type.212, (f32[128,1,128]{0,2,1:T(8,128)S(1)}, f32[1,128]{1,0:T(1,128)S(1)}, f32[1,128]{1,0:T(1,128)S(1)}) %tuple.100, (s32[]{:T(128)}, bf16[16,2,128,1,128]{4,2,3,1,0:T(8,128)(2,1)}, ...), branch_computations={%region_13.13_spmd, %region_14.17_spmd} | conditional | flops 11075843 | bytes 959580 | solution.py:298
  176.8 1.6 fusion.69
  179.7 3.0 %conditional.3 = ((f32[128,1,128]{0,2,1:T(8,128)S(1)}, f32[1,128]{1,0:T(1,128)S(1)}, f32[1,128]{1,0:T(1,128)S(1)})) conditional(s32[]{:T(128)} %convert_element_type.212, (f32[128,1,128]{0,2,1:T(8,128)S(1)}, f32[1,128]{1,0:T(1,128)S(1)}, f32[1,128]{1,0:T(1,128)S(1)}) %tuple.100, (s32[]{:T(128)}, bf16[16,2,128,1,128]{4,2,3,1,0:T(8,128)(2,1)}, ...), branch_computations={%region_13.13_spmd, %region_14.17_spmd} | conditional | flops 11075843 | bytes 959580 | solution.py:298
  179.8 1.6 fusion.69
  182.7 3.0 %conditional.3 = ((f32[128,1,128]{0,2,1:T(8,128)S(1)}, f32[1,128]{1,0:T(1,128)S(1)}, f32[1,128]{1,0:T(1,128)S(1)})) conditional(s32[]{:T(128)} %convert_element_type.212, (f32[128,1,128]{0,2,1:T(8,128)S(1)}, f32[1,128]{1,0:T(1,128)S(1)}, f32[1,128]{1,0:T(1,128)S(1)}) %tuple.100, (s32[]{:T(128)}, bf16[16,2,128,1,128]{4,2,3,1,0:T(8,128)(2,1)}, ...), branch_computations={%region_13.13_spmd, %region_14.17_spmd} | conditional | flops 11075843 | bytes 959580 | solution.py:298
  182.8 1.6 fusion.69
  185.7 3.0 %conditional.3 = ((f32[128,1,128]{0,2,1:T(8,128)S(1)}, f32[1,128]{1,0:T(1,128)S(1)}, f32[1,128]{1,0:T(1,128)S(1)})) conditional(s32[]{:T(128)} %convert_element_type.212, (f32[128,1,128]{0,2,1:T(8,128)S(1)}, f32[1,128]{1,0:T(1,128)S(1)}, f32[1,128]{1,0:T(1,128)S(1)}) %tuple.100, (s32[]{:T(128)}, bf16[16,2,128,1,128]{4,2,3,1,0:T(8,128)(2,1)}, ...), branch_computations={%region_13.13_spmd, %region_14.17_spmd} | conditional | flops 11075843 | bytes 959580 | solution.py:298
  185.8 1.6 fusion.69
  188.7 3.0 %conditional.3 = ((f32[128,1,128]{0,2,1:T(8,128)S(1)}, f32[1,128]{1,0:T(1,128)S(1)}, f32[1,128]{1,0:T(1,128)S(1)})) conditional(s32[]{:T(128)} %convert_element_type.212, (f32[128,1,128]{0,2,1:T(8,128)S(1)}, f32[1,128]{1,0:T(1,128)S(1)}, f32[1,128]{1,0:T(1,128)S(1)}) %tuple.100, (s32[]{:T(128)}, bf16[16,2,128,1,128]{4,2,3,1,0:T(8,128)(2,1)}, ...), branch_computations={%region_13.13_spmd, %region_14.17_spmd} | conditional | flops 11075843 | bytes 959580 | solution.py:298
  188.8 1.6 fusion.69
  191.8 3.0 %conditional.3 = ((f32[128,1,128]{0,2,1:T(8,128)S(1)}, f32[1,128]{1,0:T(1,128)S(1)}, f32[1,128]{1,0:T(1,128)S(1)})) conditional(s32[]{:T(128)} %convert_element_type.212, (f32[128,1,128]{0,2,1:T(8,128)S(1)}, f32[1,128]{1,0:T(1,128)S(1)}, f32[1,128]{1,0:T(1,128)S(1)}) %tuple.100, (s32[]{:T(128)}, bf16[16,2,128,1,128]{4,2,3,1,0:T(8,128)(2,1)}, ...), branch_computations={%region_13.13_spmd, %region_14.17_spmd} | conditional | flops 11075843 | bytes 959580 | solution.py:298
  191.8 1.6 fusion.69
  194.8 3.0 %conditional.3 = ((f32[128,1,128]{0,2,1:T(8,128)S(1)}, f32[1,128]{1,0:T(1,128)S(1)}, f32[1,128]{1,0:T(1,128)S(1)})) conditional(s32[]{:T(128)} %convert_element_type.212, (f32[128,1,128]{0,2,1:T(8,128)S(1)}, f32[1,128]{1,0:T(1,128)S(1)}, f32[1,128]{1,0:T(1,128)S(1)}) %tuple.100, (s32[]{:T(128)}, bf16[16,2,128,1,128]{4,2,3,1,0:T(8,128)(2,1)}, ...), branch_computations={%region_13.13_spmd, %region_14.17_spmd} | conditional | flops 11075843 | bytes 959580 | solution.py:298
  194.8 1.6 fusion.69
  197.8 3.0 %conditional.3 = ((f32[128,1,128]{0,2,1:T(8,128)S(1)}, f32[1,128]{1,0:T(1,128)S(1)}, f32[1,128]{1,0:T(1,128)S(1)})) conditional(s32[]{:T(128)} %convert_element_type.212, (f32[128,1,128]{0,2,1:T(8,128)S(1)}, f32[1,128]{1,0:T(1,128)S(1)}, f32[1,128]{1,0:T(1,128)S(1)}) %tuple.100, (s32[]{:T(128)}, bf16[16,2,128,1,128]{4,2,3,1,0:T(8,128)(2,1)}, ...), branch_computations={%region_13.13_spmd, %region_14.17_spmd} | conditional | flops 11075843 | bytes 959580 | solution.py:298
  197.8 1.6 fusion.69
  200.8 3.0 %conditional.3 = ((f32[128,1,128]{0,2,1:T(8,128)S(1)}, f32[1,128]{1,0:T(1,128)S(1)}, f32[1,128]{1,0:T(1,128)S(1)})) conditional(s32[]{:T(128)} %convert_element_type.212, (f32[128,1,128]{0,2,1:T(8,128)S(1)}, f32[1,128]{1,0:T(1,128)S(1)}, f32[1,128]{1,0:T(1,128)S(1)}) %tuple.100, (s32[]{:T(128)}, bf16[16,2,128,1,128]{4,2,3,1,0:T(8,128)(2,1)}, ...), branch_computations={%region_13.13_spmd, %region_14.17_spmd} | conditional | flops 11075843 | bytes 959580 | solution.py:298
  200.8 1.6 fusion.69
  203.8 3.0 %conditional.3 = ((f32[128,1,128]{0,2,1:T(8,128)S(1)}, f32[1,128]{1,0:T(1,128)S(1)}, f32[1,128]{1,0:T(1,128)S(1)})) conditional(s32[]{:T(128)} %convert_element_type.212, (f32[128,1,128]{0,2,1:T(8,128)S(1)}, f32[1,128]{1,0:T(1,128)S(1)}, f32[1,128]{1,0:T(1,128)S(1)}) %tuple.100, (s32[]{:T(128)}, bf16[16,2,128,1,128]{4,2,3,1,0:T(8,128)(2,1)}, ...), branch_computations={%region_13.13_spmd, %region_14.17_spmd} | conditional | flops 11075843 | bytes 959580 | solution.py:298
  203.8 1.6 fusion.69
  206.8 3.0 %conditional.3 = ((f32[128,1,128]{0,2,1:T(8,128)S(1)}, f32[1,128]{1,0:T(1,128)S(1)}, f32[1,128]{1,0:T(1,128)S(1)})) conditional(s32[]{:T(128)} %convert_element_type.212, (f32[128,1,128]{0,2,1:T(8,128)S(1)}, f32[1,128]{1,0:T(1,128)S(1)}, f32[1,128]{1,0:T(1,128)S(1)}) %tuple.100, (s32[]{:T(128)}, bf16[16,2,128,1,128]{4,2,3,1,0:T(8,128)(2,1)}, ...), branch_computations={%region_13.13_spmd, %region_14.17_spmd} | conditional | flops 11075843 | bytes 959580 | solution.py:298
  206.8 1.6 fusion.69
  212.4 1.6 fusion.133
  214.0 2.4 fusion.70
  216.5 10.2 %all-to-all-start.2 = ((bf16[8,16,2048]{2,1,0:T(8,128)(2,1)}), bf16[8,16,2048]{2,1,0:T(8,128)(2,1)S(1)}, u32[]{:S(2)}, u32[]{:S(2)}) async-start(bf16[8,16,2048]{2,1,0:T(8,128)(2,1)} %bitcast.66), calls=%async_computation.2 | async-start | bytes 1048576 | tf_op jit(solution)/shard_map/all_to_all | solution.py:88
  227.2 9.8 %all-to-all-done.2 = bf16[8,16,2048]{2,1,0:T(8,128)(2,1)S(1)} async-done(((bf16[8,16,2048]{2,1,0:T(8,128)(2,1)}), bf16[8,16,2048]{2,1,0:T(8,128)(2,1)S(1)}, u32[]{:S(2)}, u32[]{:S(2)}) %all-to-all-start.2) | async-done | bytes 524320 | tf_op jit(solution)/shard_map/all_to_all | solution.py:88
  (365 shorter events, 70.7 us)
Async XLA Ops:
  7.2 205.2 %copy-start = (bf16[128,2048]{1,0:T(8,128)(2,1)S(1)}, bf16[128,2048]{1,0:T(8,128)(2,1)}, u32[]{:S(2)}) copy-start(bf16[128,2048]{1,0:T(8,128)(2,1)} %param.48) | copy-start | bytes 1572868
  7.2 24.9 %copy-start.3 = (bf16[2048,64]{0,1:T(8,128)(2,1)S(1)}, bf16[2048,64]{0,1:T(8,128)(2,1)}, u32[]{:S(2)}) copy-start(bf16[2048,64]{0,1:T(8,128)(2,1)} %param.34) | copy-start | bytes 786436
  7.2 24.9 %copy-start.5 = (bf16[64,128]{1,0:T(8,128)(2,1)S(1)}, bf16[64,128]{1,0:T(8,128)(2,1)}, u32[]{:S(2)}) copy-start(bf16[64,128]{1,0:T(8,128)(2,1)} %param.35) | copy-start | bytes 49156
  7.2 24.9 %copy-start.7 = (f32[128]{0:T(128)S(1)}, f32[128]{0:T(128)}, u32[]{:S(2)}) copy-start(f32[128]{0:T(128)} %param.38) | copy-start | bytes 1540
  7.2 25.5 %copy-start.4 = (bf16[2048,64]{0,1:T(8,128)(2,1)S(1)}, bf16[2048,64]{0,1:T(8,128)(2,1)}, u32[]{:S(2)}) copy-start(bf16[2048,64]{0,1:T(8,128)(2,1)} %param.36) | copy-start | bytes 786436
  7.2 25.5 %copy-start.6 = (bf16[64,128]{1,0:T(8,128)(2,1)S(1)}, bf16[64,128]{1,0:T(8,128)(2,1)}, u32[]{:S(2)}) copy-start(bf16[64,128]{1,0:T(8,128)(2,1)} %param.37) | copy-start | bytes 49156
  7.2 25.5 %copy-start.8 = (f32[128]{0:T(128)S(1)}, f32[128]{0:T(128)}, u32[]{:S(2)}) copy-start(f32[128]{0:T(128)} %param.39) | copy-start | bytes 1540
  7.2 82.6 %all-gather.4.cloned.1.call-start = ((), (), s32[]{:S(2)}) async-start(), calls=%async_computation.3 | async-start | bytes 4456448 | tf_op jit(solution)/shard_map/all_gather | solution.py:34
  13.5 0.7 copy-start.2
  16.1 14.6 %all-to-all-start = ((bf16[8,128,256]{1,2,0:T(8,128)(2,1)}), bf16[8,128,256]{1,2,0:T(8,128)(2,1)S(1)}, u32[]{:S(2)}, u32[]{:S(2)}) async-start(bf16[8,128,256]{1,2,0:T(8,128)(2,1)} %broadcast_in_dim.74), calls=%async_computation | async-start | bytes 1048576 | tf_op jit(solution)/shard_map/all_to_all | solution.py:12
  20.4 144.4 %all-gather.6.cloned.1.call-start = ((), (), s32[]{:S(2)}) async-start(), calls=%async_computation.4 | async-start | bytes 1114112 | tf_op jit(solution)/shard_map/all_gather | solution.py:293
  147.6 62.3 %all-to-all-start.1 = ((bf16[16,256,64]{1,2,0:T(8,128)(2,1)}), bf16[16,256,64]{1,2,0:T(8,128)(2,1)S(1)}, u32[]{:S(2)}, u32[]{:S(2)}) async-start(bf16[16,256,64]{1,2,0:T(8,128)(2,1)} %broadcast_in_dim.107), calls=%async_computation.1 | async-start | bytes 1048576 | tf_op jit(solution)/shard_map/all_to_all | solution.py:12
  210.3 2.1 copy-start.9
  210.7 3.3 %copy-start.1 = (bf16[128,2048]{1,0:T(8,128)(2,1)S(1)}, bf16[128,2048]{1,0:T(8,128)(2,1)}, u32[]{:S(2)}) copy-start(bf16[128,2048]{1,0:T(8,128)(2,1)} %param.49) | copy-start | bytes 1572868
  216.5 20.6 %all-to-all-start.2 = ((bf16[8,16,2048]{2,1,0:T(8,128)(2,1)}), bf16[8,16,2048]{2,1,0:T(8,128)(2,1)S(1)}, u32[]{:S(2)}, u32[]{:S(2)}) async-start(bf16[8,16,2048]{2,1,0:T(8,128)(2,1)} %bitcast.66), calls=%async_computation.2 | async-start | bytes 1048576 | tf_op jit(solution)/shard_map/all_to_all | solution.py:88
Sparse Core Ops, SparseCore 0:
  14.4 75.4 all-gather.3
  93.4 71.2 all-gather.5
where the time goes:
time: 248 us; the launch traced here: 245 us
  waiting for transfers between devices  80.9 us (33%)
  matrix products  70.7 us (29%)
  other arithmetic  37.6 us (15%)
  starting transfers between devices  22.4 us (9%)
  local copies, waits for them, and re-layouts  16 us (6%)
  between operations  15.2 us (6%)
    all_gather x1, waiting for transfers between devices, in_one_piece(): lax.all_gather(both, axis, axis=dim, tiled=True)  56.6 us
    dot_general x16, matrix products, attend(): jnp.einsum('qhd,khd->hqk', query_heads, paired_piece[0], preferred_elemen...  24.5 us
    another operation x20, other arithmetic, block_pass(): jax.scipy.linalg.solve_triangular(weigh_steer + diagonal, entering, lower...  20.1 us
    dot_general x16, matrix products, attend(): jnp.einsum('hqk,khd->qhd', weights.astype(jnp.bfloat16), paired_piece[1],...  14.4 us
    all_to_all x2, starting transfers between devices, copy_for_each(): lax.all_to_all(jnp.broadcast_to(value[None], (devices, *value.shape)), ax...  12.1 us
    all_to_all x1, starting transfers between devices, sent_and_summed(): lax.all_to_all(cut_along(value, dim, devices), axis, 0, 0, tiled=True)  10.2 us
    all_to_all x1, waiting for transfers between devices, sent_and_summed(): lax.all_to_all(cut_along(value, dim, devices), axis, 0, 0, tiled=True)  9.8 us
    all_to_all x2, waiting for transfers between devices, copy_for_each(): lax.all_to_all(jnp.broadcast_to(value[None], (devices, *value.shape)), ax...  8.57 us
  transfers between devices with their start and end apart: 5, of which 4 were waited for; matrix products, arithmetic and copies ran while one was open for 44% of the time, Pallas kernels for 0%

commit v1 on v0

v1 whole, which is shorter than its diff:
```python
import jax
import jax.numpy as jnp
from jax import lax
from jax.experimental import pallas as pl
from jax.experimental.pallas import tpu as pltpu
from jax.sharding import PartitionSpec as P

HEAD_A = 64
HEAD_B = 128
ROWS = 128
GROUP = 4
F32 = jnp.float32
BF16 = jnp.bfloat16

ADJACENT = [[GROUP * a + b for b in range(GROUP)] for a in range(GROUP)]
STRIDED = [[GROUP * a + b for a in range(GROUP)] for b in range(GROUP)]
AG_ROWS = 112


def mm(a, b, dims=((1,), (0,))):
    return lax.dot_general(a, b, (dims, ((), ())), preferred_element_type=F32)


def halves(x):
    high = x.astype(BF16)
    return high, (x - high.astype(F32)).astype(BF16)


def thirds(x):
    high = x.astype(BF16)
    rest = x - high.astype(F32)
    mid = rest.astype(BF16)
    return high, mid, (rest - mid.astype(F32)).astype(BF16)


def mm3(a, b, dims=((1,), (0,))):
    ah, al = halves(a)
    bh, bl = halves(b)
    return mm(ah, bh, dims) + mm(ah, bl, dims) + mm(al, bh, dims)


def mm_left(exact, b, dims=((1,), (0,))):
    b0, b1, b2 = thirds(b)
    return mm(exact, b0, dims) + mm(exact, b1, dims) + mm(exact, b2, dims)


def mm_right(a, exact, dims=((1,), (0,))):
    a0, a1, a2 = thirds(a)
    return mm(a0, exact, dims) + mm(a1, exact, dims) + mm(a2, exact, dims)


def iotas(shape):
    return lax.broadcasted_iota(jnp.int32, shape, 0), lax.broadcasted_iota(jnp.int32, shape, 1)


def same_head():
    rows, cols = iotas((ROWS, ROWS))
    return (rows < HEAD_A) == (cols < HEAD_A)


def whole(kernel, out_shape, args, scratch=(), scalars=0):
    vmem = pl.BlockSpec(memory_space=pltpu.VMEM)
    smem = pl.BlockSpec(memory_space=pltpu.SMEM)
    many = isinstance(out_shape, (tuple, list))
    return pl.pallas_call(
        kernel,
        out_shape=out_shape,
        in_specs=[smem] * scalars + [vmem] * (len(args) - scalars),
        out_specs=[vmem] * len(out_shape) if many else vmem,
        scratch_shapes=list(scratch),
    )(*args)


def project_kernel(part_ref, x_ref, gain_ref, wa_ref, wb_ref, out_ref, own_ref, w_ref, n_ref):
    parts = out_ref.shape[0]
    pieces = x_ref.shape[0] // parts
    width = x_ref.shape[2]
    chunks = wb_ref.shape[0]
    rest = wb_ref.shape[1]
    step = AG_ROWS + rest
    for c in range(chunks):
        w_ref[step * c : step * c + AG_ROWS, :] = wa_ref[AG_ROWS * c : AG_ROWS * (c + 1), :]
        w_ref[step * c + AG_ROWS : step * (c + 1), :] = wb_ref[c]
    for p in range(parts):
        total = jnp.zeros((ROWS, width), F32)
        for t in range(pieces):
            x = x_ref[p * pieces + t].astype(F32)
            total = total + x * x
        mean = jnp.sum(total, axis=1, keepdims=True) * (1.0 / (width * pieces))
        scale = lax.rsqrt(mean + 1e-06)
        for t in range(pieces):
            at = slice(t * width, (t + 1) * width)
            x = x_ref[p * pieces + t].astype(F32)
            n_ref[:, at] = (x * scale * gain_ref[:, at]).astype(BF16)
        out_ref[p] = mm(n_ref[...], w_ref[...]).astype(BF16)

        @pl.when(part_ref[0] == p)
        def _():
            own_ref[...] = n_ref[...]


def low_rank_kernel(
    n_ref, dd_ref, rd_ref, du_ref, ru_ref, db_ref, rb_ref, shift_ref, jolt_ref, log_ref, mix_ref
):
    n = n_ref[...]
    decay_low = jnp.tanh(mm(n, dd_ref[...])).astype(BF16)
    rate_low = mm(n, rd_ref[...]).astype(BF16)
    _, cols = iotas((ROWS, ROWS))
    first = cols < HEAD_A

    def spread(ref):
        pair = ref[...]
        return jnp.where(first, pair[:, 0:1], pair[:, 1:2])

    preact = db_ref[...] + mm(decay_low, du_ref[...]) + spread(shift_ref)
    soft = jnp.maximum(-preact, 0.0) + jnp.log1p(jnp.exp(-jnp.abs(preact)))
    log_ref[...] = -jnp.exp(-soft - 0.5) - spread(jolt_ref)
    mix = rb_ref[...] + mm(rate_low, ru_ref[...])
    mix_ref[...] = 1.0 / (1.0 + jnp.exp(-mix))


def state_kernel(y_ref, log_ref, mix_ref, closing_ref, seen_ref, own_ref):
    recept = y_ref[0, :, :ROWS].astype(F32)
    keys = y_ref[0, :, ROWS:].astype(F32)
    values = y_ref[1, :, :ROWS]
    logs = log_ref[...]
    rows, cols = iotas((ROWS, ROWS))
    same = same_head()
    ones_head = jnp.where(same, 1.0, 0.0).astype(BF16)
    unit = keys * lax.rsqrt(mm_right(keys * keys, ones_head) + 1e-06)
    steer = unit * mix_ref[...]
    lower = jnp.where(rows >= cols, 1.0, 0.0).astype(BF16)
    total = mm_left(lower, logs)
    before = total - logs
    half = ROWS // 2
    top = rows < half
    center = jnp.where(
        top, total[half // 2 - 1 : half // 2], total[half + half // 2 - 1 : half + half // 2]
    )
    border = total[half - 1 : half]
    final = total[ROWS - 1 : ROWS]
    grow = jnp.exp(center - total)
    left_u = unit * jnp.exp(before - center)
    left_r = recept * jnp.exp(total - center)
    right_k = keys * grow
    right_s = steer * grow
    far_u = jnp.where(top, 0.0, unit * jnp.exp(before - border))
    far_r = jnp.where(top, 0.0, recept * jnp.exp(total - border))
    shrink = jnp.exp(border - total)
    far_k = jnp.where(top, keys * shrink, 0.0)
    far_s = jnp.where(top, steer * shrink, 0.0)
    near_right = jnp.concatenate([right_k, right_s], axis=0)
    far_right = jnp.concatenate([far_k, far_s], axis=0)
    near_left = jnp.concatenate([left_u, left_r], axis=0)
    far_left = jnp.concatenate([far_u, far_r], axis=0)
    wide_cols = lax.broadcasted_iota(jnp.int32, (2 * ROWS, ROWS), 1) < HEAD_A
    across = ((1,), (1,))
    block = (rows < half) == (cols < half)
    strict = block & (rows > cols)
    inclusive = block & (rows >= cols)
    eye = jnp.where(rows == cols, 1.0, 0.0)
    enter = unit * jnp.exp(before)
    removal = jnp.zeros((ROWS, 2 * ROWS), F32)
    seen = recept * jnp.exp(total)
    own = jnp.zeros((ROWS, ROWS), F32)
    for h in range(2):
        mine_wide = wide_cols if h == 0 else ~wide_cols
        mine = (cols < HEAD_A) if h == 0 else (cols >= HEAD_A)
        near = mm3(jnp.where(mine_wide, near_left, 0.0), near_right, across)
        far = mm3(jnp.where(mine_wide, far_left, 0.0), far_right, across)
        weigh_keys = jnp.where(strict, near[:ROWS, :ROWS], 0.0) + far[:ROWS, :ROWS]
        weigh_steer = jnp.where(strict, near[:ROWS, ROWS:], 0.0) + far[:ROWS, ROWS:]
        read_keys = jnp.where(inclusive, near[ROWS:, :ROWS], 0.0) + far[ROWS:, :ROWS]
        read_steer = jnp.where(inclusive, near[ROWS:, ROWS:], 0.0) + far[ROWS:, ROWS:]
        size = 1
        inverse = eye
        while size < ROWS:
            corner = (
                ((rows // (2 * size)) == (cols // (2 * size)))
                & ((rows // size) % 2 == 1)
                & ((cols // size) % 2 == 0)
            )
            link = jnp.where(corner, weigh_steer, 0.0)
            if size == 1:
                inverse = inverse - link
            else:
                inverse = inverse - mm3(mm3(inverse, link), inverse)
            size *= 2
        mine_values = jnp.where(mine, values, jnp.zeros_like(values))
        weighed = mm_right(weigh_keys, mine_values)
        put = jnp.concatenate([jnp.where(mine, enter, 0.0), weighed], axis=1)
        taken = mm3(inverse, put)
        removal = removal + taken
        steered = mm3(read_steer, taken)
        seen = seen - steered[:, :ROWS]
        own = own + mm_right(read_keys, mine_values) - steered[:, ROWS:]
    tail = jnp.exp(final - total)
    steer_tail = steer * tail
    down = ((0,), (0,))
    closed = mm3(removal, steer_tail, down)
    through = jnp.where(rows == cols, jnp.exp(final), 0.0) - closed[:ROWS]
    added = mm_left(values, keys * tail, down) - closed[ROWS:]
    through = jnp.where(same, through, 0.0)
    added = jnp.where(same, added, 0.0)
    through = through[:, :HEAD_A] + through[:, HEAD_A:]
    added = added[:, :HEAD_A] + added[:, HEAD_A:]
    closing_ref[...] = jnp.concatenate([through, added], axis=1).astype(BF16)
    seen_ref[...] = seen
    own_ref[...] = own


def stick_kernel(place_ref, offset_ref, kv_ref, q_ref, out_ref):
    place = place_ref[0]
    first_block = place // GROUP
    lane_block = place % GROUP
    span = GROUP * ROWS
    keys = kv_ref[:, :, :HEAD_B].reshape(span, HEAD_B)
    values = kv_ref[:, :, HEAD_B:].reshape(span, HEAD_B)
    offset = offset_ref[0]
    piece = 2 * ROWS
    rows, cols = iotas((piece, piece))
    later = jnp.where(rows >= cols, 1.0, 0.0).astype(BF16)
    ones = jnp.ones((8, span), BF16)
    across = ((1,), (1,))
    for a in range(GROUP):

        @pl.when(a < first_block)
        def _():
            out_ref[a] = jnp.zeros(out_ref.shape[1:], BF16)

        @pl.when(a >= first_block)
        def _():
            scores = mm(q_ref[a], keys, across) * (HEAD_B**-0.5) + offset
            here, there = iotas((ROWS, span))
            query_at = (a * GROUP + lane_block) * ROWS + here
            key_at = first_block * span + there
            causal = key_at < query_at
            keep = -(jnp.maximum(scores, 0.0) + jnp.log1p(jnp.exp(-jnp.abs(scores))))
            keep = jnp.where(causal, keep, 0.0)
            k0, k1, k2 = thirds(keep)

            def summed(at):
                return mm(k0[:, at], later) + mm(k1[:, at], later) + mm(k2[:, at], later)

            second = summed(slice(piece, span))
            first = summed(slice(0, piece)) + second[:, 0:1]
            sums = jnp.concatenate([first, second], axis=1)
            weights = jnp.where(causal, jnp.exp(scores + sums), 0.0)
            w0, w1, _ = thirds(weights)
            attended = mm(w0, values)
            kept = mm(ones, k0, across) + mm(ones, k1, across) + mm(ones, k2, across)
            mass = mm(ones, w0, across) + mm(ones, w1, across)
            kept0, kept1, kept2 = thirds(kept)
            mass0, mass1, _ = thirds(mass)
            line = lax.broadcasted_iota(jnp.int32, (8, ROWS), 0)
            zero = jnp.zeros((8, ROWS), BF16)
            stats = zero
            for at, row in enumerate((kept0, kept1, kept2, mass0, mass1)):
                stats = jnp.where(line == at, row, stats)
            out_ref[a, :ROWS] = attended.astype(BF16)
            out_ref[a, ROWS:] = jnp.concatenate([stats, zero], axis=0)


def finish_kernel(
    place_ref,
    closing_ref,
    seen_ref,
    own_ref,
    gate_a_ref,
    gain_ref,
    stick_ref,
    gate_b_ref,
    wa_ref,
    wb_ref,
    out_ref,
    log_ref,
):
    same = same_head()

    def spread(state):
        return jnp.where(same, jnp.concatenate([state, state], axis=1), 0.0)

    def advance(at, state):
        through = closing_ref[at, :, :HEAD_A]
        added = closing_ref[at, :, HEAD_A:].astype(F32)
        high, low = halves(spread(state))
        return mm(high, through) + mm(low, through) + added

    state = lax.fori_loop(0, place_ref[0], advance, jnp.zeros((ROWS, HEAD_A), F32))
    outputs = own_ref[...] + mm3(seen_ref[...], spread(state), ((1,), (1,)))
    ones_head = jnp.where(same, 1.0, 0.0).astype(BF16)
    centered = outputs - mm_right(outputs, ones_head) * (1.0 / HEAD_A)
    spreads = mm_right(centered * centered, ones_head) * (1.0 / HEAD_A)
    gate_a = gate_a_ref[...].astype(F32)
    normal = centered * lax.rsqrt(spreads + 0.00064)
    mixed_a = normal * gain_ref[...] * (gate_a / (1.0 + jnp.exp(-gate_a)))

    survive = jnp.zeros((1, ROWS), F32)
    mass = jnp.zeros((1, ROWS), F32)
    attended = jnp.zeros((ROWS, HEAD_B), F32)
    for a in reversed(range(GROUP)):
        stats = stick_ref[a, ROWS : ROWS + 16].astype(F32)
        factor = jnp.exp(survive)
        mass = mass + factor * (stats[3:4] + stats[4:5])
        scale = jnp.broadcast_to(factor, (ROWS, ROWS)).T
        attended = attended + scale * stick_ref[a, :ROWS].astype(F32)
        survive = survive + (stats[0:1] + stats[1:2] + stats[2:3])
    gate_b = gate_b_ref[...].astype(F32)
    mixed_b = attended * (gate_b / (1.0 + jnp.exp(-gate_b)))
    log_ref[...] = jnp.log(jnp.maximum(mass, 0.01))
    partial = mm(mixed_a.astype(BF16), wa_ref[...]) + mm(mixed_b.astype(BF16), wb_ref[...])
    out_ref[...] = partial.astype(BF16)


def sent_to_all(value, axis, groups=None):
    devices = lax.axis_size(axis) if groups is None else len(groups[0])
    return lax.all_to_all(
        jnp.broadcast_to(value[None], (devices, *value.shape)),
        axis,
        0,
        0,
        axis_index_groups=groups,
        tiled=True,
    )


def local(
    tokens,
    norm_gain,
    w_recept,
    w_key_a,
    w_value_a,
    w_gate_a,
    decay_down_weight,
    decay_up_weight,
    rate_down_weight,
    rate_up_weight,
    decay_base,
    rate_base,
    rate_shift,
    jolts,
    group_gain,
    w_query_b,
    w_key_b,
    w_value_b,
    w_gate_b,
    score_offset,
    w_out_a,
    w_out_b,
):
    part = lax.axis_index("fs")
    place = lax.axis_index("sp")
    parts = lax.axis_size("fs")
    part_at = jnp.reshape(part, (1,)).astype(jnp.int32)
    place_at = jnp.reshape(place, (1,)).astype(jnp.int32)
    row = lambda v: v.reshape(1, -1)
    shape = jax.ShapeDtypeStruct

    all_tokens = sent_to_all(tokens, ("fs", "tp"))
    piece = jnp.concatenate(
        [
            lax.select_n(part, w_recept, w_value_a, w_query_b, w_key_b),
            lax.select_n(part, w_key_a, w_gate_a, w_gate_b, w_value_b),
        ],
        axis=1,
    )
    rest = sent_to_all(piece[AG_ROWS:], "sp")
    most = lax.all_gather(piece[:AG_ROWS], "sp", axis=0, tiled=True)
    depth = norm_gain.shape[0]
    projected, normed = whole(
        project_kernel,
        (shape((parts, ROWS, 2 * ROWS), BF16), shape((ROWS, depth), BF16)),
        (part_at, all_tokens, row(norm_gain), most, rest),
        [pltpu.VMEM((depth, 2 * ROWS), BF16), pltpu.VMEM((ROWS, depth), BF16)],
        scalars=1,
    )
    mine = lax.all_to_all(projected, "fs", 0, 0, tiled=True)
    flat = shape((ROWS, ROWS), F32)
    logs, mixing = whole(
        low_rank_kernel,
        (flat, flat),
        (
            normed,
            decay_down_weight,
            rate_down_weight,
            decay_up_weight,
            rate_up_weight,
            row(decay_base),
            row(rate_base),
            rate_shift,
            jolts,
        ),
    )
    pairs = sent_to_all(mine[3], "sp", ADJACENT)
    queries = sent_to_all(mine[2, :, :ROWS], "sp", STRIDED)
    closing, seen, own = whole(
        state_kernel, (shape((ROWS, ROWS), BF16), flat, flat), (mine, logs, mixing)
    )
    closings = sent_to_all(closing, "sp")
    sticks = whole(
        stick_kernel,
        shape((GROUP, ROWS + 16, ROWS), BF16),
        (place_at, score_offset, pairs, queries),
        scalars=2,
    )
    returned = lax.all_to_all(sticks, "sp", 0, 0, axis_index_groups=STRIDED, tiled=True)
    partial, row_log = whole(
        finish_kernel,
        (shape((ROWS, w_out_a.shape[1]), BF16), shape((1, ROWS), F32)),
        (
            place_at,
            closings,
            seen,
            own,
            mine[1, :, ROWS:],
            row(group_gain),
            returned,
            mine[2, :, ROWS:],
            w_out_a,
            w_out_b,
        ),
        scalars=1,
    )
    devices = lax.axis_size("tp")
    shares = lax.all_to_all(
        partial.reshape(devices, ROWS // devices, -1), "tp", 0, 0, tiled=True
    )
    mixed = jnp.sum(shares.astype(F32), axis=0).astype(BF16)
    return mixed, row_log.reshape(ROWS, 1)


def solution(mesh):
    in_specs = (
        P(("fs", "sp"), "tp"),
        P(),
        P("sp", "tp"),
        P("sp", "tp"),
        P("sp", "tp"),
        P("sp", "tp"),
        P(),
        P(None, "tp"),
        P(),
        P(None, "tp"),
        P("tp"),
        P("tp"),
        P(("fs", "sp"), "tp"),
        P(("fs", "sp"), "tp"),
        P("tp"),
        P("sp", "tp"),
        P("sp", "tp"),
        P("sp", "tp"),
        P("sp", "tp"),
        P("tp"),
        P("tp", None),
        P("tp", None),
    )
    out_specs = (P(("fs", "sp", "tp"), None), P(("fs", "sp"), "tp"))
    return jax.shard_map(local, mesh=mesh, in_specs=in_specs, out_specs=out_specs, check_vma=False)
```

time: 248 us -> 201 us (0.81)
  the two profiles are of different devices: /device:TPU:504 before, /device:TPU:1 now
where the time goes in v1:
time: 201 us; the launch traced here: 199 us
  blocking collectives  123 us (61%)
  Pallas kernels  23.5 us (12%)
  starting transfers between devices  21.6 us (11%)
  waiting for transfers between devices  17.1 us (9%)
  local copies, waits for them, and re-layouts  10.9 us (5%)
    all_to_all x2, blocking collectives, sent_to_all(): lax.all_to_all(jnp.broadcast_to(value[None], (devices, *value.shape)), ax...  55.8 us
    all_gather x1, blocking collectives, local(): most = lax.all_gather(piece[:AG_ROWS], 'sp', axis=0, tiled=True)  30.2 us
    all_to_all x1, blocking collectives, local(): lax.all_to_all(partial.reshape(devices, ROWS // devices, -1), 'tp', 0, 0,...  26.9 us
    pallas_call x5, Pallas kernels, whole(): pl.pallas_call(kernel, out_shape=out_shape, in_specs=[smem] * scalars + [...  23.5 us
    all_to_all x3, starting transfers between devices, sent_to_all(): lax.all_to_all(jnp.broadcast_to(value[None], (devices, *value.shape)), ax...  18.3 us
    all_to_all x3, waiting for transfers between devices, sent_to_all(): lax.all_to_all(jnp.broadcast_to(value[None], (devices, *value.shape)), ax...  17.1 us
    all_to_all x1, blocking collectives, local(): mine = lax.all_to_all(projected, 'fs', 0, 0, tiled=True)  9.65 us
    unnamed x22, local copies, waits for them, and re-layouts  5.54 us
  transfers between devices with their start and end apart: 4, of which 2 were waited for; matrix products, arithmetic and copies ran while one was open for 2% of the time, Pallas kernels for 5%

profile of v1, /device:TPU:1, one launch (start us, length us, event | category | flops | bytes accessed | tf_op | source)
XLA Modules:
  0.0 198.6 jit_solution(7355759219390805722)
XLA Ops:
  0.6 0.8 select_select_fusion
  1.5 27.6 %all_to_all.40.wb_ref = bf16[16,16,256]{2,1,0:T(8,128)(2,1)} all-to-all(bf16[16,16,256]{2,1,0:T(8,128)(2,1)S(1)} %broadcast_in_dim.15), channel_id=1, replica_groups=mesh['sp'=16,'fs'=4,'tp'=8] {'sp'}, dimensions={0} | all-to-all | bytes 262144 | tf_op jit(solution)/shard_map/all_to_all | solution.py:317
  29.1 2.4 %broadcast_in_dim.14 = bf16[32,128,256]{2,1,0:T(8,128)(2,1)} broadcast(bf16[128,256]{1,0:T(8,128)(2,1)} %param.22), dimensions={1,2} | broadcast | bytes 2162688 | tf_op jit(solution)/shard_map/broadcast_in_dim | solution.py:318
  31.5 10.8 %all-to-all-start = ((bf16[32,128,256]{2,1,0:T(8,128)(2,1)}), bf16[32,128,256]{2,1,0:T(8,128)(2,1)S(1)}, u32[]{:S(2)}, u32[]{:S(2)}) async-start(bf16[32,128,256]{2,1,0:T(8,128)(2,1)} %broadcast_in_dim.14), calls=%async_computation | async-start | bytes 4194304 | tf_op jit(solution)/shard_map/all_to_all | solution.py:317
  42.4 30.2 %all_gather.3.wa_ref = bf16[1792,256]{1,0:T(8,128)(2,1)} all-gather(bf16[112,256]{1,0:T(8,128)(2,1)S(1)} %fusion), channel_id=1, replica_groups=mesh['sp'=16,'fs'=4,'tp'=8] {'sp'}, dimensions={0}, use_global_device_ids=true | all-gather | bytes 974848 | tf_op jit(solution)/shard_map/all_gather | solution.py:368
  72.6 0.0 all-to-all-done.x_ref
  72.6 0.0 copy-start
  72.6 1.3 copy-done
  73.9 4.9 %shard_map.221 = (bf16[4,128,256]{2,1,0:T(8,128)(2,1)}, bf16[128,2048]{1,0:T(8,128)(2,1)}) custom-call(s32[1]{0:T(128)} %bitcast.1.part_ref, bf16[32,128,256]{2,1,0:T(8,128)(2,1)} %copy-done, f32[1,2048]{1,0:T(1,128)} %bitcast.17, bf16[1792,256]{1,0:T(8,128)(2,1)} %all_gather.3.wa_ref, bf16[16,16,256]{2,1,0:T(8,128)(2,1)} %all_to_all.40.wb_ref), custom_call_target="tpu_custom_call" | custom-call | tf_op jit(solution)/shard_map/pallas_call | solution.py:65
  78.9 0.0 copy-start.5
  78.9 0.0 copy-start.6
  78.9 9.6 %all_to_all.41.y_ref = bf16[4,128,256]{2,1,0:T(8,128)(2,1)S(1)} all-to-all(bf16[4,128,256]{2,1,0:T(8,128)(2,1)} %get-tuple-element.11), channel_id=1, replica_groups=mesh['sp'=16,'fs'=4,'tp'=8] {'fs'}, dimensions={0} | all-to-all | bytes 524288 | tf_op jit(solution)/shard_map/all_to_all | solution.py:377
  88.5 0.0 copy-start.1
  88.5 0.0 copy-start.7
  88.5 0.0 copy-start.8
  88.5 0.6 slice_bitcast_fusion.1
  89.1 0.7 broadcast_in_dim.38
  89.8 4.0 %all-to-all-start.5 = ((bf16[4,128,128]{2,1,0:T(8,128)(2,1)}), bf16[4,128,128]{2,1,0:T(8,128)(2,1)S(1)}, u32[]{:S(2)}, u32[]{:S(2)}) async-start(bf16[4,128,128]{2,1,0:T(8,128)(2,1)} %broadcast_in_dim.38), calls=%async_computation.5 | async-start | bytes 262144 | tf_op jit(solution)/shard_map/all_to_all | solution.py:317
  93.8 12.0 %all-to-all-done.5.q_ref = bf16[4,128,128]{2,1,0:T(8,128)(2,1)S(1)} async-done(((bf16[4,128,128]{2,1,0:T(8,128)(2,1)}), bf16[4,128,128]{2,1,0:T(8,128)(2,1)S(1)}, u32[]{:S(2)}, u32[]{:S(2)}) %all-to-all-start.5) | async-done | bytes 131104 | tf_op jit(solution)/shard_map/all_to_all | solution.py:317
  105.9 0.0 copy-start.4
  105.9 0.7 broadcast_in_dim.36
  106.6 3.4 %all-to-all-start.4 = ((bf16[4,128,256]{2,1,0:T(8,128)(2,1)}), bf16[4,128,256]{2,1,0:T(8,128)(2,1)S(1)}, u32[]{:S(2)}, u32[]{:S(2)}) async-start(bf16[4,128,256]{2,1,0:T(8,128)(2,1)} %broadcast_in_dim.36), calls=%async_computation.4 | async-start | bytes 524288 | tf_op jit(solution)/shard_map/all_to_all | solution.py:317
  110.7 5.1 %all-to-all-done.4.kv_ref = bf16[4,128,256]{2,1,0:T(8,128)(2,1)S(1)} async-done(((bf16[4,128,256]{2,1,0:T(8,128)(2,1)}), bf16[4,128,256]{2,1,0:T(8,128)(2,1)S(1)}, u32[]{:S(2)}, u32[]{:S(2)}) %all-to-all-start.4) | async-done | bytes 262176 | tf_op jit(solution)/shard_map/all_to_all | solution.py:317
  115.8 0.0 copy-start.2
  115.8 0.0 copy-done.4
  115.8 0.7 copy-done.2
  116.5 5.5 %shard_map.224 = bf16[4,144,128]{2,1,0:T(8,128)(2,1)} custom-call(s32[1]{0:T(128)} %bitcast.place_ref, f32[1]{0:T(128)S(6)} %copy.28.offset_ref, bf16[4,128,256]{2,1,0:T(8,128)(2,1)} %copy-done.2, bf16[4,128,128]{2,1,0:T(8,128)(2,1)} %copy-done.4), custom_call_target="tpu_custom_call" | custom-call | tf_op jit(solution)/shard_map/pallas_call | solution.py:65
  122.0 3.3 %all-to-all-start.6 = ((bf16[4,144,128]{2,1,0:T(8,128)(2,1)}), bf16[4,144,128]{2,1,0:T(8,128)(2,1)S(1)}, u32[]{:S(2)}, u32[]{:S(2)}) async-start(bf16[4,144,128]{2,1,0:T(8,128)(2,1)} %shard_map.224), calls=%async_computation.6 | async-start | bytes 294912 | tf_op jit(solution)/shard_map/all_to_all | solution.py:406
  125.3 0.0 copy-done.5
  125.3 1.0 copy.24.dd_ref
  126.3 0.0 copy-done.6
  126.3 1.0 copy.25.rd_ref
  127.3 0.0 copy-done.7
  127.3 0.7 copy.26.shift_ref
  128.1 0.0 copy-done.8
  128.1 0.7 copy.27.jolt_ref
  128.8 2.6 %shard_map.222 = (f32[128,128]{1,0:T(8,128)}, f32[128,128]{1,0:T(8,128)}) custom-call(bf16[128,2048]{1,0:T(8,128)(2,1)} %get-tuple-element.12.n_ref, bf16[2048,64]{1,0:T(8,128)(2,1)} %copy.24.dd_ref, bf16[2048,64]{1,0:T(8,128)(2,1)} %copy.25.rd_ref, bf16[64,128]{1,0:T(8,128)(2,1)} %du_ref.1, bf16[64,128]{1,0:T(8,128)(2,1)} %ru_ref.1, f32[1,128]{1,0:T(1,128)} %bitcast.18, ...), custom_call_target="tpu_custom_call" | custom-call | tf_op jit(solution)/shard_map/pallas_call | solution.py:65
  131.4 0.0 copy-done.1
  131.4 7.2 %shard_map.223 = (bf16[128,128]{1,0:T(8,128)(2,1)}, f32[128,128]{1,0:T(8,128)}, f32[128,128]{1,0:T(8,128)}) custom-call(bf16[4,128,256]{2,1,0:T(8,128)(2,1)} %copy-done.1, f32[128,128]{1,0:T(8,128)} %get-tuple-element.13.log_ref, f32[128,128]{1,0:T(8,128)} %get-tuple-element.14.mix_ref), custom_call_target="tpu_custom_call" | custom-call | tf_op jit(solution)/shard_map/pallas_call | solution.py:65
  138.7 0.0 all-to-all-done.6.stick_ref
  138.7 0.0 copy-start.3
  138.7 0.9 broadcast_in_dim.16
  139.5 28.2 %all_to_all.42.closing_ref = bf16[16,128,128]{2,1,0:T(8,128)(2,1)} all-to-all(bf16[16,128,128]{2,1,0:T(8,128)(2,1)S(1)} %broadcast_in_dim.16), channel_id=1, replica_groups=mesh['sp'=16,'fs'=4,'tp'=8] {'sp'}, dimensions={0} | all-to-all | bytes 1048576 | tf_op jit(solution)/shard_map/all_to_all | solution.py:317
  167.7 0.0 copy-done.3
  167.7 3.3 %shard_map.225 = (bf16[128,2048]{1,0:T(8,128)(2,1)}, f32[1,128]{1,0:T(1,128)}) custom-call(s32[1]{0:T(128)} %bitcast.place_ref, bf16[16,128,128]{2,1,0:T(8,128)(2,1)} %all_to_all.42.closing_ref, f32[128,128]{1,0:T(8,128)} %get-tuple-element.16.seen_ref, f32[128,128]{1,0:T(8,128)} %get-tuple-element.17.own_ref, ...), custom_call_target="tpu_custom_call" | custom-call | tf_op jit(solution)/shard_map/pallas_call | solution.py:65
  171.0 26.9 %all_to_all.43 = bf16[8,16,2048]{2,1,0:T(8,128)(2,1)S(1)} all-to-all(bf16[8,16,2048]{2,1,0:T(8,128)(2,1)} %bitcast.16), channel_id=1, replica_groups=mesh['sp'=16,'fs'=4,'tp'=8] {'tp'}, dimensions={0} | all-to-all | bytes 1048576 | tf_op jit(solution)/shard_map/all_to_all | solution.py:425
  197.9 0.7 reduce_sum.12
  (4 shorter events, 0.0 us)
Async XLA Ops:
  31.5 41.0 %all-to-all-start = ((bf16[32,128,256]{2,1,0:T(8,128)(2,1)}), bf16[32,128,256]{2,1,0:T(8,128)(2,1)S(1)}, u32[]{:S(2)}, u32[]{:S(2)}) async-start(bf16[32,128,256]{2,1,0:T(8,128)(2,1)} %broadcast_in_dim.14), calls=%async_computation | async-start | bytes 4194304 | tf_op jit(solution)/shard_map/all_to_all | solution.py:317
  72.6 1.3 copy-start
  78.9 46.5 %copy-start.5 = (bf16[2048,64]{0,1:T(8,128)(2,1)S(1)}, bf16[2048,64]{0,1:T(8,128)(2,1)}, u32[]{:S(2)}) copy-start(bf16[2048,64]{0,1:T(8,128)(2,1)} %param.28) | copy-start | bytes 786436
  78.9 47.5 %copy-start.6 = (bf16[2048,64]{0,1:T(8,128)(2,1)S(1)}, bf16[2048,64]{0,1:T(8,128)(2,1)}, u32[]{:S(2)}) copy-start(bf16[2048,64]{0,1:T(8,128)(2,1)} %param.30) | copy-start | bytes 786436
  88.5 42.9 %copy-start.1 = (bf16[4,128,256]{2,1,0:T(8,128)(2,1)}, bf16[4,128,256]{2,1,0:T(8,128)(2,1)S(1)}, u32[]{:S(2)}) copy-start(bf16[4,128,256]{2,1,0:T(8,128)(2,1)S(1)} %all_to_all.41.y_ref) | copy-start | bytes 786436
  88.5 38.8 %copy-start.7 = (f32[128,2]{0,1:T(2,128)S(1)}, f32[128,2]{0,1:T(2,128)}, u32[]{:S(2)}) copy-start(f32[128,2]{0,1:T(2,128)} %param.34) | copy-start | bytes 3076
  88.5 39.6 %copy-start.8 = (f32[128,2]{0,1:T(2,128)S(1)}, f32[128,2]{0,1:T(2,128)}, u32[]{:S(2)}) copy-start(f32[128,2]{0,1:T(2,128)} %param.35) | copy-start | bytes 3076
  89.8 16.1 %all-to-all-start.5 = ((bf16[4,128,128]{2,1,0:T(8,128)(2,1)}), bf16[4,128,128]{2,1,0:T(8,128)(2,1)S(1)}, u32[]{:S(2)}, u32[]{:S(2)}) async-start(bf16[4,128,128]{2,1,0:T(8,128)(2,1)} %broadcast_in_dim.38), calls=%async_computation.5 | async-start | bytes 262144 | tf_op jit(solution)/shard_map/all_to_all | solution.py:317
  105.9 9.9 %copy-start.4 = (bf16[4,128,128]{2,1,0:T(8,128)(2,1)}, bf16[4,128,128]{2,1,0:T(8,128)(2,1)S(1)}, u32[]{:S(2)}) copy-start(bf16[4,128,128]{2,1,0:T(8,128)(2,1)S(1)} %all-to-all-done.5.q_ref) | copy-start | bytes 393220
  106.6 9.2 %all-to-all-start.4 = ((bf16[4,128,256]{2,1,0:T(8,128)(2,1)}), bf16[4,128,256]{2,1,0:T(8,128)(2,1)S(1)}, u32[]{:S(2)}, u32[]{:S(2)}) async-start(bf16[4,128,256]{2,1,0:T(8,128)(2,1)} %broadcast_in_dim.36), calls=%async_computation.4 | async-start | bytes 524288 | tf_op jit(solution)/shard_map/all_to_all | solution.py:317
  115.8 0.7 copy-start.2
  122.0 16.7 %all-to-all-start.6 = ((bf16[4,144,128]{2,1,0:T(8,128)(2,1)}), bf16[4,144,128]{2,1,0:T(8,128)(2,1)S(1)}, u32[]{:S(2)}, u32[]{:S(2)}) async-start(bf16[4,144,128]{2,1,0:T(8,128)(2,1)} %shard_map.224), calls=%async_computation.6 | async-start | bytes 294912 | tf_op jit(solution)/shard_map/all_to_all | solution.py:406
  138.7 29.0 %copy-start.3 = (bf16[4,144,128]{2,1,0:T(8,128)(2,1)}, bf16[4,144,128]{2,1,0:T(8,128)(2,1)S(1)}, u32[]{:S(2)}) copy-start(bf16[4,144,128]{2,1,0:T(8,128)(2,1)S(1)} %all-to-all-done.6.stick_ref) | copy-start | bytes 442372

commit v2 on v1

--- a/solution.py
+++ b/solution.py
@@ -14,7 +14,8 @@
 
 ADJACENT = [[GROUP * a + b for b in range(GROUP)] for a in range(GROUP)]
 STRIDED = [[GROUP * a + b for a in range(GROUP)] for b in range(GROUP)]
-AG_ROWS = 112
+PARITY = [[2 * i + p for i in range(8)] for p in range(2)]
+LIMIT = 16 * 1024 * 1024
 
 
 def mm(a, b, dims=((1,), (0,))):
@@ -68,19 +69,15 @@
         in_specs=[smem] * scalars + [vmem] * (len(args) - scalars),
         out_specs=[vmem] * len(out_shape) if many else vmem,
         scratch_shapes=list(scratch),
+        compiler_params=pltpu.CompilerParams(vmem_limit_bytes=LIMIT),
     )(*args)
 
 
-def project_kernel(part_ref, x_ref, gain_ref, wa_ref, wb_ref, out_ref, own_ref, w_ref, n_ref):
-    parts = out_ref.shape[0]
+def near_kernel(place_ref, part_ref, x_ref, gain_ref, w_ref, n_ref, acc_ref, own_ref):
+    parts = n_ref.shape[1] // ROWS
     pieces = x_ref.shape[0] // parts
     width = x_ref.shape[2]
-    chunks = wb_ref.shape[0]
-    rest = wb_ref.shape[1]
-    step = AG_ROWS + rest
-    for c in range(chunks):
-        w_ref[step * c : step * c + AG_ROWS, :] = wa_ref[AG_ROWS * c : AG_ROWS * (c + 1), :]
-        w_ref[step * c + AG_ROWS : step * (c + 1), :] = wb_ref[c]
+    half = width // 2
     for p in range(parts):
         total = jnp.zeros((ROWS, width), F32)
         for t in range(pieces):
@@ -89,28 +86,50 @@
         mean = jnp.sum(total, axis=1, keepdims=True) * (1.0 / (width * pieces))
         scale = lax.rsqrt(mean + 1e-06)
         for t in range(pieces):
-            at = slice(t * width, (t + 1) * width)
             x = x_ref[p * pieces + t].astype(F32)
-            n_ref[:, at] = (x * scale * gain_ref[:, at]).astype(BF16)
-        out_ref[p] = mm(n_ref[...], w_ref[...]).astype(BF16)
-
-        @pl.when(part_ref[0] == p)
-        def _():
-            own_ref[...] = n_ref[...]
+            gain = gain_ref[:, t * width : (t + 1) * width]
+            normed = (x * scale * gain).astype(BF16)
+            rows = slice(p * ROWS, (p + 1) * ROWS)
+            at = slice(t * half, (t + 1) * half)
+            n_ref[0, rows, at] = normed[:, :half]
+            n_ref[1, rows, at] = normed[:, half:]
+    acc_ref[...] = mm(n_ref[place_ref[0] % 2], w_ref[...])
+    own_ref[...] = n_ref[:, pl.ds(pl.multiple_of(part_ref[0] * ROWS, ROWS), ROWS)]
+
+
+def far_kernel(place_ref, n_ref, acc_ref, w_ref, out_ref):
+    both = acc_ref[...] + mm(n_ref[1 - place_ref[0] % 2], w_ref[...])
+    out_ref[...] = both.astype(BF16).reshape(out_ref.shape)
 
 
 def low_rank_kernel(
-    n_ref, dd_ref, rd_ref, du_ref, ru_ref, db_ref, rb_ref, shift_ref, jolt_ref, log_ref, mix_ref
+    n_ref,
+    dd_ref,
+    rd_ref,
+    du_ref,
+    ru_ref,
+    db_ref,
+    rb_ref,
+    shift_ref,
+    jolt_ref,
+    log_ref,
+    mix_ref,
 ):
-    n = n_ref[...]
-    decay_low = jnp.tanh(mm(n, dd_ref[...])).astype(BF16)
-    rate_low = mm(n, rd_ref[...]).astype(BF16)
-    _, cols = iotas((ROWS, ROWS))
-    first = cols < HEAD_A
+    downs = jnp.concatenate([dd_ref[...], rd_ref[...]], axis=0)
+    low = jnp.zeros((ROWS, downs.shape[0]), F32)
+    for p in range(2):
+        steps = range(p * ROWS, downs.shape[1], 2 * ROWS)
+        chosen = jnp.concatenate([downs[:, c : c + ROWS] for c in steps], axis=1)
+        low = low + mm(n_ref[p], chosen, ((1,), (1,)))
+    rank = dd_ref.shape[0]
+    decay_low = jnp.tanh(low[:, :rank]).astype(BF16)
+    rate_low = low[:, rank:].astype(BF16)
+    heads, _ = iotas((ROWS, ROWS))
 
     def spread(ref):
         pair = ref[...]
-        return jnp.where(first, pair[:, 0:1], pair[:, 1:2])
+        lines = jnp.where(heads < HEAD_A, pair[0:1], pair[1:2])
+        return lines.T
 
     preact = db_ref[...] + mm(decay_low, du_ref[...]) + spread(shift_ref)
     soft = jnp.maximum(-preact, 0.0) + jnp.log1p(jnp.exp(-jnp.abs(preact)))
@@ -119,7 +138,7 @@
     mix_ref[...] = 1.0 / (1.0 + jnp.exp(-mix))
 
 
-def state_kernel(y_ref, log_ref, mix_ref, closing_ref, seen_ref, own_ref):
+def state_kernel(y_ref, log_ref, mix_ref, send_ref, seen_ref, own_ref):
     recept = y_ref[0, :, :ROWS].astype(F32)
     keys = y_ref[0, :, ROWS:].astype(F32)
     values = y_ref[1, :, :ROWS]
@@ -204,18 +223,43 @@
     added = jnp.where(same, added, 0.0)
     through = through[:, :HEAD_A] + through[:, HEAD_A:]
     added = added[:, :HEAD_A] + added[:, HEAD_A:]
-    closing_ref[...] = jnp.concatenate([through, added], axis=1).astype(BF16)
+    closing = jnp.concatenate([through, added], axis=1).astype(BF16)
+    for g in range(send_ref.shape[0]):
+        send_ref[g, :, : 2 * ROWS] = y_ref[3]
+        send_ref[g, :, 2 * ROWS :] = closing
     seen_ref[...] = seen
     own_ref[...] = own
 
 
-def stick_kernel(place_ref, offset_ref, kv_ref, q_ref, out_ref):
+def spread_heads(state):
+    return jnp.where(same_head(), jnp.concatenate([state, state], axis=1), 0.0)
+
+
+def stick_kernel(place_ref, offset_ref, near_ref, q_ref, out_ref, prefix_ref):
     place = place_ref[0]
     first_block = place // GROUP
     lane_block = place % GROUP
     span = GROUP * ROWS
-    keys = kv_ref[:, :, :HEAD_B].reshape(span, HEAD_B)
-    values = kv_ref[:, :, HEAD_B:].reshape(span, HEAD_B)
+    keys = near_ref[:, :, :ROWS].reshape(span, HEAD_B)
+    values = near_ref[:, :, ROWS : 2 * ROWS].reshape(span, HEAD_B)
+    rows, cols = iotas((ROWS, HEAD_A))
+    through = jnp.where(rows % HEAD_A == cols, 1.0, 0.0)
+    added = jnp.zeros((ROWS, HEAD_A), F32)
+    for g in range(GROUP):
+
+        @pl.when(lane_block == g)
+        def _():
+            prefix_ref[...] = jnp.concatenate([through, added], axis=1)
+
+        step = near_ref[g, :, 2 * ROWS : 2 * ROWS + HEAD_A]
+        both = jnp.concatenate([spread_heads(through), spread_heads(added)], axis=0)
+        high, low = halves(both)
+        both = mm(high, step) + mm(low, step)
+        through = both[:ROWS]
+        added = both[ROWS:] + near_ref[g, :, 2 * ROWS + HEAD_A :].astype(F32)
+    closing = jnp.concatenate([through, added], axis=1).astype(BF16)
+    for g in range(GROUP):
+        out_ref[g, ROWS + 16 :] = closing
     offset = offset_ref[0]
     piece = 2 * ROWS
     rows, cols = iotas((piece, piece))
@@ -226,7 +270,7 @@
 
         @pl.when(a < first_block)
         def _():
-            out_ref[a] = jnp.zeros(out_ref.shape[1:], BF16)
+            out_ref[a, : ROWS + 16] = jnp.zeros((ROWS + 16, ROWS), BF16)
 
         @pl.when(a >= first_block)
         def _():
@@ -258,40 +302,38 @@
             for at, row in enumerate((kept0, kept1, kept2, mass0, mass1)):
                 stats = jnp.where(line == at, row, stats)
             out_ref[a, :ROWS] = attended.astype(BF16)
-            out_ref[a, ROWS:] = jnp.concatenate([stats, zero], axis=0)
+            out_ref[a, ROWS : ROWS + 16] = jnp.concatenate([stats, zero], axis=0)
 
 
 def finish_kernel(
     place_ref,
-    closing_ref,
+    stick_ref,
+    prefix_ref,
     seen_ref,
     own_ref,
-    gate_a_ref,
+    y_ref,
     gain_ref,
-    stick_ref,
-    gate_b_ref,
     wa_ref,
     wb_ref,
     out_ref,
     log_ref,
 ):
     same = same_head()
-
-    def spread(state):
-        return jnp.where(same, jnp.concatenate([state, state], axis=1), 0.0)
-
-    def advance(at, state):
-        through = closing_ref[at, :, :HEAD_A]
-        added = closing_ref[at, :, HEAD_A:].astype(F32)
-        high, low = halves(spread(state))
-        return mm(high, through) + mm(low, through) + added
-
-    state = lax.fori_loop(0, place_ref[0], advance, jnp.zeros((ROWS, HEAD_A), F32))
-    outputs = own_ref[...] + mm3(seen_ref[...], spread(state), ((1,), (1,)))
+    group = place_ref[0] // GROUP
+    state = jnp.zeros((ROWS, HEAD_A), F32)
+    for a in range(GROUP - 1):
+        step = stick_ref[a, ROWS + 16 :]
+        high, low = halves(spread_heads(state))
+        moved = mm(high, step[:, :HEAD_A]) + mm(low, step[:, :HEAD_A])
+        moved = moved + step[:, HEAD_A:].astype(F32)
+        state = jnp.where(a < group, moved, state)
+    prefix = prefix_ref[...]
+    state = mm3(spread_heads(state), prefix[:, :HEAD_A]) + prefix[:, HEAD_A:]
+    outputs = own_ref[...] + mm3(seen_ref[...], spread_heads(state), ((1,), (1,)))
     ones_head = jnp.where(same, 1.0, 0.0).astype(BF16)
     centered = outputs - mm_right(outputs, ones_head) * (1.0 / HEAD_A)
     spreads = mm_right(centered * centered, ones_head) * (1.0 / HEAD_A)
-    gate_a = gate_a_ref[...].astype(F32)
+    gate_a = y_ref[1, :, ROWS:].astype(F32)
     normal = centered * lax.rsqrt(spreads + 0.00064)
     mixed_a = normal * gain_ref[...] * (gate_a / (1.0 + jnp.exp(-gate_a)))
 
@@ -305,7 +347,7 @@
         scale = jnp.broadcast_to(factor, (ROWS, ROWS)).T
         attended = attended + scale * stick_ref[a, :ROWS].astype(F32)
         survive = survive + (stats[0:1] + stats[1:2] + stats[2:3])
-    gate_b = gate_b_ref[...].astype(F32)
+    gate_b = y_ref[2, :, ROWS:].astype(F32)
     mixed_b = attended * (gate_b / (1.0 + jnp.exp(-gate_b)))
     log_ref[...] = jnp.log(jnp.maximum(mass, 0.01))
     partial = mm(mixed_a.astype(BF16), wa_ref[...]) + mm(mixed_b.astype(BF16), wb_ref[...])
@@ -364,14 +406,24 @@
         ],
         axis=1,
     )
-    rest = sent_to_all(piece[AG_ROWS:], "sp")
-    most = lax.all_gather(piece[:AG_ROWS], "sp", axis=0, tiled=True)
+    near = lax.all_gather(piece, "sp", axis=0, axis_index_groups=PARITY, tiled=True)
+    swap = [(i, i ^ 1) for i in range(lax.axis_size("sp"))]
+    far = lax.ppermute(near, "sp", swap)
     depth = norm_gain.shape[0]
-    projected, normed = whole(
-        project_kernel,
-        (shape((parts, ROWS, 2 * ROWS), BF16), shape((ROWS, depth), BF16)),
-        (part_at, all_tokens, row(norm_gain), most, rest),
-        [pltpu.VMEM((depth, 2 * ROWS), BF16), pltpu.VMEM((ROWS, depth), BF16)],
+    normed, partial, own_normed = whole(
+        near_kernel,
+        (
+            shape((2, parts * ROWS, depth // 2), BF16),
+            shape((parts * ROWS, 2 * ROWS), F32),
+            shape((2, ROWS, depth // 2), BF16),
+        ),
+        (place_at, part_at, all_tokens, row(norm_gain), near),
+        scalars=2,
+    )
+    projected = whole(
+        far_kernel,
+        shape((parts, ROWS, 2 * ROWS), BF16),
+        (place_at, normed, partial, far),
         scalars=1,
     )
     mine = lax.all_to_all(projected, "fs", 0, 0, tiled=True)
@@ -380,45 +432,33 @@
         low_rank_kernel,
         (flat, flat),
         (
-            normed,
-            decay_down_weight,
-            rate_down_weight,
+            own_normed,
+            decay_down_weight.T,
+            rate_down_weight.T,
             decay_up_weight,
             rate_up_weight,
             row(decay_base),
             row(rate_base),
-            rate_shift,
-            jolts,
+            rate_shift.T,
+            jolts.T,
         ),
     )
-    pairs = sent_to_all(mine[3], "sp", ADJACENT)
     queries = sent_to_all(mine[2, :, :ROWS], "sp", STRIDED)
-    closing, seen, own = whole(
-        state_kernel, (shape((ROWS, ROWS), BF16), flat, flat), (mine, logs, mixing)
-    )
-    closings = sent_to_all(closing, "sp")
-    sticks = whole(
+    send, seen, own = whole(
+        state_kernel, (shape((GROUP, ROWS, 3 * ROWS), BF16), flat, flat), (mine, logs, mixing)
+    )
+    around = lax.all_to_all(send, "sp", 0, 0, axis_index_groups=ADJACENT, tiled=True)
+    sticks, prefix = whole(
         stick_kernel,
-        shape((GROUP, ROWS + 16, ROWS), BF16),
-        (place_at, score_offset, pairs, queries),
+        (shape((GROUP, 2 * ROWS + 16, ROWS), BF16), flat),
+        (place_at, score_offset, around, queries),
         scalars=2,
     )
     returned = lax.all_to_all(sticks, "sp", 0, 0, axis_index_groups=STRIDED, tiled=True)
     partial, row_log = whole(
         finish_kernel,
         (shape((ROWS, w_out_a.shape[1]), BF16), shape((1, ROWS), F32)),
-        (
-            place_at,
-            closings,
-            seen,
-            own,
-            mine[1, :, ROWS:],
-            row(group_gain),
-            returned,
-            mine[2, :, ROWS:],
-            w_out_a,
-            w_out_b,
-        ),
+        (place_at, returned, prefix, seen, own, mine, row(group_gain), w_out_a, w_out_b),
         scalars=1,
     )
     devices = lax.axis_size("tp")

time: 201 us -> 149 us (0.74)
  blocking collectives: 123 us -> 82.7 us
  local copies, waits for them, and re-layouts: 10.9 us -> 3.21 us
  Pallas kernels: 23.5 us -> 17 us
  waiting for transfers between devices: 17.1 us -> 19.7 us
    all_to_all x2 -> x1, blocking collectives: 55.8 us -> 17.4 us  [local(): lax.all_to_all(sticks, 'sp', 0, 0, axis_index_groups=STRIDED, tiled=True)]
    all_to_all x3 -> x2, waiting for transfers between devices: 17.1 us -> 5.19 us  [sent_to_all(): lax.all_to_all(jnp.broadcast_to(value[None], (devices, *value.shape)), ax...]
    all_to_all x1, waiting for transfers between devices: 0.01 us -> 7.43 us  [local(): lax.all_to_all(send, 'sp', 0, 0, axis_index_groups=ADJACENT, tiled=True)]
    ppermute x0 -> x1, waiting for transfers between devices: none -> 7.07 us  [local(): far = lax.ppermute(near, 'sp', swap)]
    pallas_call x5 -> x6, Pallas kernels: 23.5 us -> 17 us  [whole(): pl.pallas_call(kernel, out_shape=out_shape, in_specs=[smem] * scalars + [...]
    unnamed x22 -> x40, local copies, waits for them, and re-layouts: 5.54 us -> 0.11 us
    all_to_all x1, blocking collectives: 26.9 us -> 24 us  [local(): lax.all_to_all(partial.reshape(devices, ROWS // devices, -1), 'tp', 0, 0,...]
    ppermute x0 -> x1, starting transfers between devices: none -> 2.58 us  [local(): far = lax.ppermute(near, 'sp', swap)]
  transfers between devices with their start and end apart: 4 -> 4, of which waited for: 2 -> 3; matrix products, arithmetic and copies ran while one was open for 2% -> 0% of each run, Pallas kernels for 5% -> 6%
where the time goes in v2:
time: 149 us; the launch traced here: 148 us
  blocking collectives  82.7 us (56%)
  starting transfers between devices  22.9 us (15%)
  waiting for transfers between devices  19.7 us (13%)
  Pallas kernels  17 us (11%)
  local copies, waits for them, and re-layouts  3.21 us (2%)
  between operations  1.59 us (1%)
    all_gather x1, blocking collectives, local(): lax.all_gather(piece, 'sp', axis=0, axis_index_groups=PARITY, tiled=True)  31 us
    all_to_all x1, blocking collectives, local(): lax.all_to_all(partial.reshape(devices, ROWS // devices, -1), 'tp', 0, 0,...  24 us
    all_to_all x1, blocking collectives, local(): lax.all_to_all(sticks, 'sp', 0, 0, axis_index_groups=STRIDED, tiled=True)  17.4 us
    pallas_call x6, Pallas kernels, whole(): pl.pallas_call(kernel, out_shape=out_shape, in_specs=[smem] * scalars + [...  17 us
    all_to_all x2, starting transfers between devices, sent_to_all(): lax.all_to_all(jnp.broadcast_to(value[None], (devices, *value.shape)), ax...  16.3 us
    all_to_all x1, blocking collectives, local(): mine = lax.all_to_all(projected, 'fs', 0, 0, tiled=True)  10.5 us
    all_to_all x1, waiting for transfers between devices, local(): lax.all_to_all(send, 'sp', 0, 0, axis_index_groups=ADJACENT, tiled=True)  7.43 us
    ppermute x1, waiting for transfers between devices, local(): far = lax.ppermute(near, 'sp', swap)  7.07 us
  transfers between devices with their start and end apart: 4, of which 3 were waited for; matrix products, arithmetic and copies ran while one was open for 0% of the time, Pallas kernels for 6%

profile of v2, /device:TPU:1, one launch (start us, length us, event | category | flops | bytes accessed | tf_op | source)
XLA Modules:
  0.0 147.9 jit_solution(12343001579299473346)
XLA Ops:
  0.6 2.4 %broadcast_in_dim.6 = bf16[32,128,256]{2,1,0:T(8,128)(2,1)} broadcast(bf16[128,256]{1,0:T(8,128)(2,1)} %param.22), dimensions={1,2} | broadcast | bytes 2162688 | tf_op jit(solution)/shard_map/broadcast_in_dim | solution.py:360
  3.1 0.0 copy-start.16
  3.1 0.0 copy-start.17
  3.1 0.0 copy-start.18
  3.1 0.0 copy-start.19
  3.1 0.0 copy-start.6
  3.1 10.6 %all-to-all-start = ((bf16[32,128,256]{2,1,0:T(8,128)(2,1)}), bf16[32,128,256]{2,1,0:T(8,128)(2,1)S(1)}, u32[]{:S(2)}, u32[]{:S(2)}) async-start(bf16[32,128,256]{2,1,0:T(8,128)(2,1)} %broadcast_in_dim.6), calls=%async_computation | async-start | bytes 4194304 | tf_op jit(solution)/shard_map/all_to_all | solution.py:359
  13.8 0.0 copy-done.12
  13.8 0.0 copy-done.13
  13.8 0.0 copy-done.14
  13.8 0.0 copy-done.15
  13.8 0.0 copy-done.16
  13.8 0.0 copy-done.17
  13.9 0.0 copy-done.18
  13.9 0.0 copy-done.19
  13.9 31.0 %all_gather.3.w_ref = bf16[1024,256]{1,0:T(8,128)(2,1)S(1)} all-gather(bf16[128,256]{1,0:T(8,128)(2,1)S(1)} %pad_maximum_fusion), channel_id=1, replica_groups={{0,64,128,192,256,320,384,448},{32,96,160,224,288,352,416,480},{1,65,12..., dimensions={0}, use_global_device_ids=true | all-gather | bytes 589824 | tf_op jit(solution)/shard_map/all_gather | solution.py:409
  44.9 2.6 %collective-permute-start = (bf16[1024,256]{1,0:T(8,128)(2,1)S(1)}, bf16[1024,256]{1,0:T(8,128)(2,1)}, u32[]{:S(2)}, u32[]{:S(2)}) collective-permute-start(bf16[1024,256]{1,0:T(8,128)(2,1)S(1)} %all_gather.3.w_ref), channel_id=1, source_target_pairs={{0,32},{32,0},{64,96},{96,64},{128,160},{160,128},{192,224},{224,1... | collective-permute-start | bytes 1572872 | tf_op jit(solution)/shard_map/ppermute | solution.py:411
  47.5 0.0 all-to-all-done.x_ref
  47.5 0.0 copy-done.6
  47.5 1.5 %shard_map.221 = (bf16[2,512,1024]{2,1,0:T(8,128)(2,1)S(1)}, f32[512,256]{1,0:T(8,128)S(1)}, bf16[2,128,1024]{2,1,0:T(8,128)(2,1)S(1)}) custom-call(s32[1]{0:T(128)} %bitcast.place_ref, s32[1]{0:T(128)} %bitcast.1.part_ref, bf16[32,128,256]{2,1,0:T(8,128)(2,1)S(1)} %all-to-all-done.x_ref, f32[1,2048]{1,0:T(1,128)S(1)} %bitcast.17, ...), custom_call_target="tpu_custom_call" | custom-call | tf_op jit(solution)/shard_map/pallas_call | solution.py:66
  49.0 7.1 %collective-permute-done.w_ref = bf16[1024,256]{1,0:T(8,128)(2,1)} collective-permute-done((bf16[1024,256]{1,0:T(8,128)(2,1)S(1)}, bf16[1024,256]{1,0:T(8,128)(2,1)}, u32[]{:S(2)}, u32[]{:S(2)}) %collective-permute-start) | collective-permute-done | bytes 524320 | tf_op jit(solution)/shard_map/ppermute | solution.py:411
  56.1 0.0 copy-start.7
  56.1 0.0 copy-start.8
  56.1 0.0 copy-start.9
  56.1 0.0 copy-start.10
  56.1 1.5 %shard_map.222 = bf16[4,128,256]{2,1,0:T(8,128)(2,1)S(1)} custom-call(s32[1]{0:T(128)} %bitcast.place_ref, bf16[2,512,1024]{2,1,0:T(8,128)(2,1)S(1)} %get-tuple-element.14.n_ref, f32[512,256]{1,0:T(8,128)S(1)} %get-tuple-element.15.acc_ref, bf16[1024,256]{1,0:T(8,128)(2,1)} %collective-permute-done.w_ref), custom_call_target="tpu_custom_call" | custom-call | tf_op jit(solution)/shard_map/pallas_call | solution.py:66
  57.6 0.0 copy-start
  57.7 0.0 copy-start.1
  57.7 0.0 copy-start.11
  57.7 10.5 %all_to_all.30.y_ref = bf16[4,128,256]{2,1,0:T(8,128)(2,1)S(1)} all-to-all(bf16[4,128,256]{2,1,0:T(8,128)(2,1)S(1)} %shard_map.222), channel_id=1, replica_groups=mesh['sp'=16,'fs'=4,'tp'=8] {'fs'}, dimensions={0} | all-to-all | bytes 524288 | tf_op jit(solution)/shard_map/all_to_all | solution.py:429
  68.1 0.7 broadcast_in_dim.15
  68.8 5.7 %all-to-all-start.3 = ((bf16[4,128,128]{2,1,0:T(8,128)(2,1)}), bf16[4,128,128]{2,1,0:T(8,128)(2,1)S(1)}, u32[]{:S(2)}, u32[]{:S(2)}) async-start(bf16[4,128,128]{2,1,0:T(8,128)(2,1)} %broadcast_in_dim.15), calls=%async_computation.3 | async-start | bytes 262144 | tf_op jit(solution)/shard_map/all_to_all | solution.py:359
  74.5 0.0 copy-done.2
  74.5 0.0 copy-done.3
  74.5 0.0 copy-done.4
  74.5 0.0 copy-done.5
  74.5 0.0 copy-done.7
  74.5 0.5 shard_map.223
  75.1 6.4 %shard_map.224 = (bf16[4,128,384]{2,1,0:T(8,128)(2,1)}, f32[128,128]{1,0:T(8,128)S(1)}, f32[128,128]{1,0:T(8,128)S(1)}) custom-call(bf16[4,128,256]{2,1,0:T(8,128)(2,1)S(1)} %all_to_all.30.y_ref, f32[128,128]{1,0:T(8,128)S(1)} %get-tuple-element.17.log_ref, f32[128,128]{1,0:T(8,128)S(1)} %get-tuple-element.18.mix_ref), custom_call_target="tpu_custom_call" | custom-call | tf_op jit(solution)/shard_map/pallas_call | solution.py:66
  81.5 5.2 %all-to-all-done.3.q_ref = bf16[4,128,128]{2,1,0:T(8,128)(2,1)S(1)} async-done(((bf16[4,128,128]{2,1,0:T(8,128)(2,1)}), bf16[4,128,128]{2,1,0:T(8,128)(2,1)S(1)}, u32[]{:S(2)}, u32[]{:S(2)}) %all-to-all-start.3) | async-done | bytes 131104 | tf_op jit(solution)/shard_map/all_to_all | solution.py:359
  86.7 4.0 %all-to-all-start.2 = ((bf16[4,128,384]{2,1,0:T(8,128)(2,1)}), bf16[4,128,384]{2,1,0:T(8,128)(2,1)S(1)}, u32[]{:S(2)}, u32[]{:S(2)}) async-start(bf16[4,128,384]{2,1,0:T(8,128)(2,1)} %get-tuple-element.19), calls=%async_computation.2 | async-start | bytes 786432 | tf_op jit(solution)/shard_map/all_to_all | solution.py:450
  91.4 7.4 %all-to-all-done.2.near_ref = bf16[4,128,384]{2,1,0:T(8,128)(2,1)S(1)} async-done(((bf16[4,128,384]{2,1,0:T(8,128)(2,1)}), bf16[4,128,384]{2,1,0:T(8,128)(2,1)S(1)}, u32[]{:S(2)}, u32[]{:S(2)}) %all-to-all-start.2) | async-done | bytes 393248 | tf_op jit(solution)/shard_map/all_to_all | solution.py:450
  98.8 4.9 %shard_map.225 = (bf16[4,272,128]{2,1,0:T(8,128)(2,1)S(1)}, f32[128,128]{1,0:T(8,128)S(1)}) custom-call(s32[1]{0:T(128)} %bitcast.place_ref, f32[1]{0:T(128)S(6)} %copy.24.offset_ref, bf16[4,128,384]{2,1,0:T(8,128)(2,1)S(1)} %all-to-all-done.2.near_ref, bf16[4,128,128]{2,1,0:T(8,128)(2,1)S(1)} %all-to-all-done.3.q_ref), custom_call_target="tpu_custom_call" | custom-call | tf_op jit(solution)/shard_map/pallas_call | solution.py:66
  103.8 17.4 %all_to_all.31.stick_ref = bf16[4,272,128]{2,1,0:T(8,128)(2,1)S(1)} all-to-all(bf16[4,272,128]{2,1,0:T(8,128)(2,1)S(1)} %get-tuple-element.20), channel_id=1, replica_groups={{0,128,256,384},{32,160,288,416},{64,192,320,448},{96,224,352,480},{1,1..., dimensions={0} | all-to-all | bytes 557056 | tf_op jit(solution)/shard_map/all_to_all | solution.py:457
  121.1 0.0 copy-done.11
  121.1 2.1 %shard_map.226 = (bf16[128,2048]{1,0:T(8,128)(2,1)S(1)}, f32[1,128]{1,0:T(1,128)}) custom-call(s32[1]{0:T(128)} %bitcast.place_ref, bf16[4,272,128]{2,1,0:T(8,128)(2,1)S(1)} %all_to_all.31.stick_ref, f32[128,128]{1,0:T(8,128)S(1)} %get-tuple-element.21.prefix_ref, f32[128,128]{1,0:T(8,128)S(1)} %get-tuple-element.22.seen_ref, ...), custom_call_target="tpu_custom_call" | custom-call | tf_op jit(solution)/shard_map/pallas_call | solution.py:66
  123.3 24.0 %all_to_all.32 = bf16[8,16,2048]{2,1,0:T(8,128)(2,1)S(1)} all-to-all(bf16[8,16,2048]{2,1,0:T(8,128)(2,1)S(1)} %bitcast.14), channel_id=1, replica_groups=mesh['sp'=16,'fs'=4,'tp'=8] {'tp'}, dimensions={0} | all-to-all | bytes 1048576 | tf_op jit(solution)/shard_map/all_to_all | solution.py:465
  147.2 0.7 reduce_sum.12
  (16 shorter events, 0.1 us)
Async XLA Ops:
  3.1 10.7 %copy-start.12 = (bf16[128,128]{1,0:T(8,128)(2,1)S(1)}, bf16[128,128]{1,0:T(8,128)(2,1)}, u32[]{:S(2)}) copy-start(bf16[128,128]{1,0:T(8,128)(2,1)} %param.40) | copy-start | bytes 98308
  3.1 10.7 %copy-start.13 = (bf16[128,128]{1,0:T(8,128)(2,1)S(1)}, bf16[128,128]{1,0:T(8,128)(2,1)}, u32[]{:S(2)}) copy-start(bf16[128,128]{1,0:T(8,128)(2,1)} %param.39) | copy-start | bytes 98308
  3.1 10.8 %copy-start.14 = (bf16[128,128]{1,0:T(8,128)(2,1)S(1)}, bf16[128,128]{1,0:T(8,128)(2,1)}, u32[]{:S(2)}) copy-start(bf16[128,128]{1,0:T(8,128)(2,1)} %param.25) | copy-start | bytes 98308
  3.1 10.8 %copy-start.15 = (bf16[128,128]{1,0:T(8,128)(2,1)S(1)}, bf16[128,128]{1,0:T(8,128)(2,1)}, u32[]{:S(2)}) copy-start(bf16[128,128]{1,0:T(8,128)(2,1)} %param.27) | copy-start | bytes 98308
  3.1 10.8 %copy-start.16 = (bf16[128,128]{1,0:T(8,128)(2,1)S(1)}, bf16[128,128]{1,0:T(8,128)(2,1)}, u32[]{:S(2)}) copy-start(bf16[128,128]{1,0:T(8,128)(2,1)} %param.37) | copy-start | bytes 98308
  3.1 10.8 %copy-start.17 = (bf16[128,128]{1,0:T(8,128)(2,1)S(1)}, bf16[128,128]{1,0:T(8,128)(2,1)}, u32[]{:S(2)}) copy-start(bf16[128,128]{1,0:T(8,128)(2,1)} %param.38) | copy-start | bytes 98308
  3.1 10.8 %copy-start.18 = (bf16[128,128]{1,0:T(8,128)(2,1)S(1)}, bf16[128,128]{1,0:T(8,128)(2,1)}, u32[]{:S(2)}) copy-start(bf16[128,128]{1,0:T(8,128)(2,1)} %param.24) | copy-start | bytes 98308
  3.1 10.8 %copy-start.19 = (bf16[128,128]{1,0:T(8,128)(2,1)S(1)}, bf16[128,128]{1,0:T(8,128)(2,1)}, u32[]{:S(2)}) copy-start(bf16[128,128]{1,0:T(8,128)(2,1)} %param.26) | copy-start | bytes 98308
  3.1 44.4 %copy-start.6 = (f32[2048]{0:T(1024)S(1)}, f32[2048]{0:T(1024)}, u32[]{:S(2)}) copy-start(f32[2048]{0:T(1024)} %param.23) | copy-start | bytes 24580
  3.1 44.3 %all-to-all-start = ((bf16[32,128,256]{2,1,0:T(8,128)(2,1)}), bf16[32,128,256]{2,1,0:T(8,128)(2,1)S(1)}, u32[]{:S(2)}, u32[]{:S(2)}) async-start(bf16[32,128,256]{2,1,0:T(8,128)(2,1)} %broadcast_in_dim.6), calls=%async_computation | async-start | bytes 4194304 | tf_op jit(solution)/shard_map/all_to_all | solution.py:359
  44.9 11.2 %collective-permute-start = (bf16[1024,256]{1,0:T(8,128)(2,1)S(1)}, bf16[1024,256]{1,0:T(8,128)(2,1)}, u32[]{:S(2)}, u32[]{:S(2)}) collective-permute-start(bf16[1024,256]{1,0:T(8,128)(2,1)S(1)} %all_gather.3.w_ref), channel_id=1, source_target_pairs={{0,32},{32,0},{64,96},{96,64},{128,160},{160,128},{192,224},{224,1... | collective-permute-start | bytes 1572872 | tf_op jit(solution)/shard_map/ppermute | solution.py:411
  56.0 18.4 %copy-start.2 = (bf16[2048,64]{0,1:T(8,128)(2,1)S(1)}, bf16[2048,64]{0,1:T(8,128)(2,1)}, u32[]{:S(2)}) copy-start(bf16[2048,64]{0,1:T(8,128)(2,1)} %param.28) | copy-start | bytes 786436
  56.1 18.4 %copy-start.3 = (bf16[2048,64]{0,1:T(8,128)(2,1)S(1)}, bf16[2048,64]{0,1:T(8,128)(2,1)}, u32[]{:S(2)}) copy-start(bf16[2048,64]{0,1:T(8,128)(2,1)} %param.30) | copy-start | bytes 786436
  56.1 18.4 %copy-start.4 = (bf16[64,128]{1,0:T(8,128)(2,1)S(1)}, bf16[64,128]{1,0:T(8,128)(2,1)}, u32[]{:S(2)}) copy-start(bf16[64,128]{1,0:T(8,128)(2,1)} %du_ref.1) | copy-start | bytes 49156
  56.1 18.4 %copy-start.5 = (bf16[64,128]{1,0:T(8,128)(2,1)S(1)}, bf16[64,128]{1,0:T(8,128)(2,1)}, u32[]{:S(2)}) copy-start(bf16[64,128]{1,0:T(8,128)(2,1)} %ru_ref.1) | copy-start | bytes 49156
  56.1 18.4 %copy-start.7 = (f32[128,2]{0,1:T(2,128)S(1)}, f32[128,2]{0,1:T(2,128)}, u32[]{:S(2)}) copy-start(f32[128,2]{0,1:T(2,128)} %param.34) | copy-start | bytes 3076
  56.1 18.4 %copy-start.8 = (f32[128,2]{0,1:T(2,128)S(1)}, f32[128,2]{0,1:T(2,128)}, u32[]{:S(2)}) copy-start(f32[128,2]{0,1:T(2,128)} %param.35) | copy-start | bytes 3076
  56.1 18.4 %copy-start.9 = (f32[128]{0:T(128)S(1)}, f32[128]{0:T(128)}, u32[]{:S(2)}) copy-start(f32[128]{0:T(128)} %param.32) | copy-start | bytes 1540
  56.1 18.4 %copy-start.10 = (f32[128]{0:T(128)S(1)}, f32[128]{0:T(128)}, u32[]{:S(2)}) copy-start(f32[128]{0:T(128)} %param.33) | copy-start | bytes 1540
  57.6 63.5 %copy-start = (bf16[128,2048]{1,0:T(8,128)(2,1)S(1)}, bf16[128,2048]{1,0:T(8,128)(2,1)}, u32[]{:S(2)}) copy-start(bf16[128,2048]{1,0:T(8,128)(2,1)} %wa_ref.1) | copy-start | bytes 1572868
  57.7 63.5 %copy-start.1 = (bf16[128,2048]{1,0:T(8,128)(2,1)S(1)}, bf16[128,2048]{1,0:T(8,128)(2,1)}, u32[]{:S(2)}) copy-start(bf16[128,2048]{1,0:T(8,128)(2,1)} %wb_ref.1) | copy-start | bytes 1572868
  57.7 63.5 %copy-start.11 = (f32[128]{0:T(128)S(1)}, f32[128]{0:T(128)}, u32[]{:S(2)}) copy-start(f32[128]{0:T(128)} %param.36) | copy-start | bytes 1540
  68.8 17.9 %all-to-all-start.3 = ((bf16[4,128,128]{2,1,0:T(8,128)(2,1)}), bf16[4,128,128]{2,1,0:T(8,128)(2,1)S(1)}, u32[]{:S(2)}, u32[]{:S(2)}) async-start(bf16[4,128,128]{2,1,0:T(8,128)(2,1)} %broadcast_in_dim.15), calls=%async_computation.3 | async-start | bytes 262144 | tf_op jit(solution)/shard_map/all_to_all | solution.py:359
  86.7 12.1 %all-to-all-start.2 = ((bf16[4,128,384]{2,1,0:T(8,128)(2,1)}), bf16[4,128,384]{2,1,0:T(8,128)(2,1)S(1)}, u32[]{:S(2)}, u32[]{:S(2)}) async-start(bf16[4,128,384]{2,1,0:T(8,128)(2,1)} %get-tuple-element.19), calls=%async_computation.2 | async-start | bytes 786432 | tf_op jit(solution)/shard_map/all_to_all | solution.py:450
